TPU v7x, 32 devices: a whole 2x2x4 slice. The times are simulated.
32 devices in a mesh: ep: 8 (over z, y), tp: 4 (over x, core).
Axes of the slice: x: 2, y: 2, z: 4, core: 2. Of those that a mesh axis runs over, the one named last changes fastest.
Arguments:
- tokens: bfloat16 [192, 2048], P('ep'), may hold values from -6 to 6
- norm_attn: float32 [2048], replicated, may hold values from 0.1 to 1.9
- w_query: bfloat16 [2048, 2048], P(None, 'tp'), may hold values from -0.125 to 0.125
- w_key: bfloat16 [2048, 256], P(None, 'tp'), may hold values from -0.125 to 0.125
- w_value: bfloat16 [2048, 256], P(None, 'tp'), may hold values from -0.125 to 0.125
- w_out: bfloat16 [2048, 2048], P('tp'), may hold values from -1 to 1
- head_bias: float32 [32], P('tp'), may hold values from -7 to -3
- key_cache: bfloat16 [192, 4, 1024, 64], P('ep', 'tp'), may hold values from -6 to 6
- value_cache: bfloat16 [192, 4, 1024, 64], P('ep', 'tp'), may hold values from -6 to 6
- lengths: int32 [192], P('ep'), may hold values from 1 to 1024, 98304 in all
- norm_ffn: float32 [2048], replicated, may hold values from 0.1 to 1.9
- w_group: bfloat16 [2048, 4], replicated, may hold values from -0.125 to 0.125
- w_fine: bfloat16 [2048, 8], replicated, may hold values from -0.125 to 0.125
- routes: int32 [192, 2], P('ep'), may hold values from 0 to 7, as said below
- e_gate: bfloat16 [8, 2048, 512], P('ep', 'tp'), may hold values from -0.125 to 0.125
- e_up: bfloat16 [8, 2048, 512], P('ep', 'tp'), may hold values from -0.125 to 0.125
- e_down: bfloat16 [8, 512, 2048], P('ep', None, 'tp'), may hold values from -1 to 1
- d_gate: bfloat16 [2048, 8192], P('tp', 'ep'), may hold values from -0.125 to 0.125
- d_up: bfloat16 [2048, 8192], P('tp', 'ep'), may hold values from -0.125 to 0.125
- d_down: bfloat16 [8192, 2048], P('ep', 'tp'), may hold values from -0.25 to 0.25
- w_mix: float32 [2048], replicated, may hold values from -0.125 to 0.125
Outputs:
- mixed: bfloat16 [192, 2048], P('ep', 'tp')
- new_keys: bfloat16 [192, 4, 64], P('ep', 'tp')
- new_values: bfloat16 [192, 4, 64], P('ep', 'tp')
Inputs may be any that keep to these rules, and one draw needn't show every extreme that they name: `routes`: the 2 experts of a row are distinct and lie in one group of 2 consecutive experts. Among the rows of one device each expert is named at most 12 times. One group, the same on every device, is named by exactly 12 rows of every device, so that each of its experts is named exactly 12 times by every device.
All inputs are finite; a program needn't handle non-finite values. No bound on the sum of `lengths` on one device may be relied on, other than what follows from the above.
Results may differ from a plain program's by a relative error of at most 0.019.
Values may be sent and summed in bfloat16 or wider, within the bound.
A program may use at most 128 MiB of HBM per device.

v0:
```python
import jax
import jax.numpy as jnp
from jax import lax
from jax.sharding import PartitionSpec as P

GROUPS = 4
TOP_K = 2


norm_eps = 1e-06
segment_len = 128


def normed(values, gains):
    wide = values.astype(jnp.float32)
    return wide * lax.rsqrt(jnp.mean(wide * wide, axis=-1, keepdims=True) + norm_eps) * gains


def suffix_sums(terms):
    length = terms.shape[-1]
    pieces = length // segment_len
    shaped = terms.reshape(terms.shape[:-1] + (pieces, segment_len))
    inner = lax.iota(jnp.int32, segment_len)
    later_inner = (inner[:, None] > inner[None, :]).astype(jnp.float32)
    within = jnp.einsum("...ij,jk->...ik", shaped, later_inner, precision=lax.Precision.HIGHEST)
    outer = lax.iota(jnp.int32, pieces)
    later_outer = (outer[:, None] > outer[None, :]).astype(jnp.float32)
    carried = jnp.einsum(
        "...i,ij->...j", jnp.sum(shaped, axis=-1), later_outer, precision=lax.Precision.HIGHEST
    )
    return (within + carried[..., None]).reshape(terms.shape)


def stick_read(queries, keys, values, lengths, bias_table):
    scores = jnp.einsum("bkgd,bksd->bkgs", queries, keys, preferred_element_type=jnp.float32)
    scores = scores * queries.shape[-1] ** (-0.5) + bias_table[None, :, :, None]
    positions = lax.iota(jnp.int32, keys.shape[2])
    inside = (positions[None, :] < lengths[:, None])[:, None, None, :]
    fails = jnp.where(inside, jax.nn.log_sigmoid(-scores), 0.0)
    weights = jnp.where(inside, jnp.exp(jax.nn.log_sigmoid(scores) + suffix_sums(fails)), 0.0)
    result = jnp.einsum(
        "bkgs,bksd->bkgd", weights.astype(jnp.bfloat16), values, preferred_element_type=jnp.float32
    )
    return result.astype(jnp.bfloat16).reshape(queries.shape[0], -1)


def route_weights(group_logits, fine_logits, chosen, per_group):
    group_iota = lax.iota(jnp.int32, group_logits.shape[1])
    own_group = chosen[:, 0] // per_group
    own_logit = jnp.sum(
        jnp.where(group_iota[None, :] == own_group[:, None], group_logits, 0.0), axis=1
    )
    group_share = 1.0 / jnp.sum(jnp.exp(group_logits - own_logit[:, None]), axis=1)
    expert_iota = lax.iota(jnp.int32, fine_logits.shape[1])
    picked = jnp.sum(
        jnp.where(expert_iota[None, None, :] == chosen[:, :, None], fine_logits[:, None, :], 0.0),
        axis=2,
    )
    within = 1.0 / jnp.sum(jnp.exp(picked[:, None, :] - picked[:, :, None]), axis=2)
    return group_share[:, None] * within


def slot_ranks(flat_routes):
    count = flat_routes.shape[0]
    same_expert = flat_routes[:, None] == flat_routes[None, :]
    position = lax.iota(jnp.int32, count)
    earlier = position[None, :] < position[:, None]
    return jnp.sum(same_expert & earlier, axis=1)


def shards(
    tokens,
    norm_attn,
    w_query,
    w_key,
    w_value,
    w_out,
    head_bias,
    key_cache,
    value_cache,
    lengths,
    norm_ffn,
    w_group,
    w_fine,
    routes,
    e_gate,
    e_up,
    e_down,
    d_gate,
    d_up,
    d_down,
    w_mix,
):
    seq_count = tokens.shape[0]
    width_part = d_gate.shape[0]
    dense_units = d_gate.shape[1]
    expert_units = e_gate.shape[2]
    kv_local = key_cache.shape[1]
    head_dim = key_cache.shape[3]
    ep_size = lax.axis_size("ep")
    per_group = ep_size // GROUPS
    capacity = max(2, (seq_count + per_group - 1) // per_group)
    h_first = normed(tokens, norm_attn).astype(jnp.bfloat16)
    queries = jnp.dot(h_first, w_query, preferred_element_type=jnp.float32).astype(jnp.bfloat16)
    new_keys = jnp.dot(h_first, w_key, preferred_element_type=jnp.float32).astype(jnp.bfloat16)
    new_values = jnp.dot(h_first, w_value, preferred_element_type=jnp.float32).astype(jnp.bfloat16)
    grouped = queries.reshape(seq_count, kv_local, -1, head_dim)
    heads_out = stick_read(
        grouped, key_cache, value_cache, lengths, head_bias.reshape(kv_local, -1)
    )
    partial_value = jnp.dot(heads_out, w_out, preferred_element_type=jnp.float32).astype(
        jnp.bfloat16
    )
    attended = lax.psum(
        lax.optimization_barrier(partial_value).astype(jnp.float32).astype(jnp.bfloat16), "tp"
    ).astype(jnp.float32)
    resid = tokens.astype(jnp.float32) + attended
    h_second = normed(resid, norm_ffn).astype(jnp.bfloat16)
    column = lax.axis_index("tp") * width_part
    h_slice = lax.dynamic_slice_in_dim(h_second, column, width_part, 1)
    resid_slice = lax.dynamic_slice_in_dim(resid, column, width_part, 1)
    dense_in = jnp.concatenate([d_gate, d_up], axis=1)
    expert_in = jnp.concatenate([e_gate[0], e_up[0]], axis=1)
    every_row = lax.all_gather(h_slice, "ep", axis=0, tiled=True)
    every_route = lax.all_gather(routes, "ep", axis=0, tiled=True)
    own_expert = lax.axis_index("ep")
    route_blocks = every_route.reshape(ep_size, seq_count * TOP_K)
    block_ranks = jax.vmap(slot_ranks)(route_blocks)
    capacity_iota = lax.iota(jnp.int32, capacity)
    hits = route_blocks == own_expert
    picks = hits[:, None, :] & (block_ranks[:, None, :] == capacity_iota[None, :, None])
    pick_rows = jnp.sum(
        picks.astype(jnp.int32).reshape(ep_size, capacity, seq_count, TOP_K), axis=3
    )
    chosen_rows = (
        jnp.einsum(
            "sct,std->scd",
            pick_rows.astype(jnp.bfloat16),
            every_row.reshape(ep_size, seq_count, width_part),
            preferred_element_type=jnp.float32,
        )
        .astype(jnp.bfloat16)
        .reshape(-1, width_part)
    )
    group_slice = lax.dynamic_slice_in_dim(w_group, column, width_part, 0)
    fine_slice = lax.dynamic_slice_in_dim(w_fine, column, width_part, 0)
    mix_slice = lax.dynamic_slice_in_dim(w_mix, column, width_part, 0)
    partials = (
        jnp.dot(every_row, dense_in, preferred_element_type=jnp.float32),
        jnp.dot(every_row, group_slice, preferred_element_type=jnp.float32),
        jnp.dot(every_row, fine_slice, preferred_element_type=jnp.float32),
        jnp.dot(every_row.astype(jnp.float32), mix_slice, precision=lax.Precision.HIGHEST),
        jnp.dot(chosen_rows, expert_in, preferred_element_type=jnp.float32),
    )
    dense_pre, group_logits, fine_logits, mix_logit, expert_pre = (
        lax.psum(partials[0].astype(jnp.bfloat16), "tp").astype(jnp.float32),
        lax.psum(partials[1].astype(jnp.bfloat16), "tp").astype(jnp.float32),
        lax.psum(partials[2].astype(jnp.bfloat16), "tp").astype(jnp.float32),
        lax.psum(partials[3].astype(jnp.bfloat16), "tp").astype(jnp.float32),
        lax.psum(partials[4].astype(jnp.bfloat16), "tp").astype(jnp.float32),
    )
    shares = route_weights(group_logits, fine_logits, every_route, per_group)
    mix_gate = jax.nn.sigmoid(mix_logit)
    expert_hidden = (
        jax.nn.silu(expert_pre[:, :expert_units]) * expert_pre[:, expert_units:]
    ).astype(jnp.bfloat16)
    expert_out = jnp.dot(expert_hidden, e_down[0], preferred_element_type=jnp.float32).astype(
        jnp.bfloat16
    )
    own_share = jnp.sum(
        jnp.where(hits, shares.reshape(ep_size, -1), 0.0).reshape(ep_size, seq_count, TOP_K), axis=2
    )
    slot_share = jnp.sum(pick_rows.astype(jnp.float32) * own_share[:, None, :], axis=2).reshape(-1)
    weighted_out = expert_out.astype(jnp.float32) * slot_share[:, None]
    token_iota = lax.iota(jnp.int32, seq_count)
    source_iota = lax.iota(jnp.int32, ep_size)
    filled = jnp.sum(pick_rows, axis=2)
    local_token = jnp.sum(pick_rows * token_iota[None, None, :], axis=2)
    slot_token = jnp.where(filled > 0, source_iota[:, None] * seq_count + local_token, -1).reshape(
        -1
    )
    dense_hidden = (jax.nn.silu(dense_pre[:, :dense_units]) * dense_pre[:, dense_units:]).astype(
        jnp.bfloat16
    )
    rows_here = lax.iota(jnp.int32, lax.axis_size("ep") * seq_count)
    select = (rows_here[:, None] == slot_token[None, :]).astype(jnp.float32)
    expert_part = jnp.dot(select, weighted_out, precision=lax.Precision.HIGHEST)
    dense_part = jnp.dot(dense_hidden, d_down, preferred_element_type=jnp.float32)
    mixed = resid_slice + lax.psum_scatter(
        expert_part + mix_gate[:, None] * dense_part, "ep", scatter_dimension=0, tiled=True
    )
    return (
        mixed.astype(jnp.bfloat16),
        new_keys.reshape(seq_count, kv_local, head_dim),
        new_values.reshape(seq_count, kv_local, head_dim),
    )


def solution(mesh):
    placed = (
        P("ep", None),
        P(),
        P(None, "tp"),
        P(None, "tp"),
        P(None, "tp"),
        P("tp", None),
        P("tp"),
        P("ep", "tp", None, None),
        P("ep", "tp", None, None),
        P("ep"),
        P(),
        P(),
        P(),
        P("ep", None),
        P("ep", "tp", None),
        P("ep", "tp", None),
        P("ep", None, "tp"),
        P("tp", "ep"),
        P("tp", "ep"),
        P("ep", "tp"),
        P(),
    )
    return jax.shard_map(
        shards,
        mesh=mesh,
        in_specs=placed,
        out_specs=(P("ep", "tp"), P("ep", "tp", None), P("ep", "tp", None)),
        check_vma=False,
    )
```

profile of v0, /device:TPU:0, one launch (start us, length us, event | category | flops | bytes accessed | tf_op | source)
XLA Modules:
  0.0 217.9 jit_solution(6778820421968040462)
XLA Ops:
  7.2 0.0 copy-start
  7.2 0.0 all-reduce.5.cloned.1.call-start
  7.2 1.2 fusion.39
  8.4 2.1 convolution_convert_fusion.5
  10.5 0.1 reshape.204
  10.7 0.1 iota_compare_fusion.2
  10.8 0.5 fusion.10
  11.3 0.9 copy-done.1
  12.2 1.4 fusion.68
  13.6 0.1 copy.60
  13.7 0.1 fusion.56
  13.9 0.1 copy.61
  14.0 2.6 %convolution_add_fusion = f32[24,8,8,128]{3,2,1,0:T(8,128)} fusion(f32[24,8,8,128]{3,1,2,0:T(8,128)} %get-tuple-element.13, f32[24,8,8]{2,1,0:T(8,128)S(1)} %copy.61), kind=kOutput, calls=%fused_computation.11 | convolution fusion | flops 302202880 | bytes 1579008 | tf_op jit(solution)/shard_map/...ij,jk->...ik/dot_general | solution.py:25
  16.6 2.1 reshape.207
  18.7 3.3 %fusion.15 = bf16[24,8,64]{2,1,0:T(8,128)(2,1)S(1)} fusion(bf16[24,1,1024,64]{2,3,1,0:T(8,128)(2,1)} %param.29, f32[24,8,1024]{2,1,0:T(8,128)} %reshape.207, f32[24,8,1024]{2,1,0:T(8,128)} %copy-done.1, pred[24,1024]{1,0:T(8,128)(4,1)S(1)} %iota_compare_fusion.2), kind=kOutput, calls=%fused_computation.21 | convolution fusion | flops 27340800 | bytes 4767744 | tf_op jit(solution)/shard_map/bkgs,bksd->bkgd/dot_general | solution.py:41
  22.0 0.1 reshape.209
  22.1 2.6 %convolution_convert_fusion.1 = bf16[24,2048]{1,0:T(8,128)(2,1)} fusion(bf16[24,512]{1,0:T(8,128)(2,1)S(1)} %reshape.209, bf16[512,2048]{1,0:T(8,128)(2,1)} %param.26), kind=kOutput, calls=%fused_computation.7 | convolution fusion | flops 50380800 | bytes 2220032 | tf_op jit(solution)/shard_map/dot_general | solution.py:111
  24.8 0.0 all-reduce.5.cloned.1.call-update
  24.8 0.0 all-reduce.7.cloned.1.call-start
  24.8 22.3 %all-gather = s32[8,24,2]{1,2,0:T(2,128)S(1)} all-gather(s32[1,24,2]{1,2,0:T(2,128)S(1)} %bitcast.67), channel_id=1, replica_groups=mesh['ep'=8,'tp'=4] {'ep'}, dimensions={0}, use_global_device_ids=true | all-gather | bytes 1728 | tf_op jit(solution)/shard_map/all_gather | solution.py:125
  47.2 0.1 copy.63
  47.3 0.1 reshape.215
  47.4 0.1 copy.64
  47.4 0.3 convert_reduce_fusion
  47.8 0.8 dynamic-slice
  48.5 0.8 dynamic_slice.19
  49.3 0.1 copy.66
  49.4 0.1 copy.67
  49.4 9.9 %all-reduce.5.cloned.1.call-done = bf16[24,2048]{1,0:T(8,128)(2,1)} async-done(((bf16[24,2048]{1,0:T(8,128)(2,1)}), bf16[24,2048]{1,0:T(8,128)(2,1)}) %all-reduce.5.cloned.1.call-update) | async-done | bytes 98320 | tf_op jit(solution)/shard_map/psum | solution.py:114
  59.3 1.0 multiply_reduce_fusion
  60.4 0.7 copy-done.3
  61.0 0.1 multiply_convert_fusion
  61.1 30.8 %all_gather.7 = bf16[192,512]{1,0:T(8,128)(2,1)S(1)} all-gather(bf16[24,512]{1,0:T(8,128)(2,1)S(1)} %multiply_convert_fusion), channel_id=1, replica_groups=mesh['ep'=8,'tp'=4] {'ep'}, dimensions={0}, use_global_device_ids=true | all-gather | bytes 221184 | tf_op jit(solution)/shard_map/all_gather | solution.py:124
  91.9 0.8 convolution_convert_fusion.8
  92.7 0.3 fusion.70
  93.0 0.9 convolution_convert_fusion.9
  93.9 5.9 %all-reduce = (bf16[192]{0:T(256)(128)(2,1)S(1)}, bf16[192,8]{0,1:T(8,128)(2,1)S(1)}, bf16[192,4]{0,1:T(4,128)(2,1)S(1)}) all-reduce(bf16[192]{0:T(256)(128)(2,1)S(1)} %convert_element_type.122, bf16[192,8]{0,1:T(8,128)(2,1)S(1)} %convolution_convert_fusion.8, ...), channel_id=1, replica_groups=mesh['ep'=8,'tp'=4] {'tp'}, use_global_device_ids=true, to_apply=%region_17.18 | all-reduce | flops 2496 | bytes 9984 | tf_op jit(solution)/shard_map/psum | solution.py:159
  99.9 0.1 eq.90
  100.0 0.3 convert_reduce_fusion.2
  100.3 0.3 multiply_reduce_fusion.2
  100.6 0.8 convolution_convert_fusion.3
  101.4 1.6 reshape.211
  103.0 3.1 %convolution_convert_fusion = bf16[192,2048]{1,0:T(8,128)(2,1)} fusion(bf16[192,512]{1,0:T(8,128)(2,1)S(1)} %all_gather.7, bf16[512,1024]{1,0:T(8,128)(2,1)} %param.39, bf16[512,1024]{1,0:T(8,128)(2,1)} %param.38), kind=kOutput, calls=%fused_computation.4 | convolution fusion | flops 407240704 | bytes 3080192 | tf_op jit(solution)/shard_map/dot_general | solution.py:149
  106.1 1.0 convolution_convert_fusion.2
  107.0 0.0 all-reduce.7.cloned.1.call-update
  107.1 0.0 reduce-scatter.2.cloned.1.call-start
  107.1 0.1 copy.68
  107.2 0.1 select_n.63
  107.3 0.1 mul.137
  107.4 0.1 multiply_reduce_fusion.1
  107.5 0.1 copy.70
  107.6 0.1 mul.140
  107.6 35.4 %all-reduce.7.cloned.1.call-done = (bf16[192,2048]{1,0:T(8,128)(2,1)}, bf16[96,1024]{1,0:T(8,128)(2,1)}) async-done(((bf16[192,2048]{1,0:T(8,128)(2,1)}, bf16[96,1024]{1,0:T(8,128)(2,1)}), (bf16[192,2048]{1,0:T(8,128)(2,1)}, bf16[96,1024]{1,0:T(8,128)(2,1)})) %all-reduce.7.cloned.1.call-update) | async-done | bytes 983056 | tf_op jit(solution)/shard_map/psum | solution.py:156
  143.1 1.1 convert_element_type.113
  144.1 1.3 convert_element_type.125
  145.5 0.2 fusion.14
  145.7 0.0 copy-start.5
  145.7 0.4 convolution_multiply_fusion
  146.1 1.1 convolution_add_fusion.1
  147.2 0.0 reduce-scatter.2.cloned.1.call-update
  147.2 1.8 fusion.18
  149.0 1.8 fusion.19
  150.8 59.1 %reduce-scatter.2.cloned.1.call-done = f32[24,512]{1,0:T(8,128)} async-done(((f32[192,512]{1,0:T(8,128)}), f32[24,512]{1,0:T(8,128)}) %reduce-scatter.2.cloned.1.call-update) | async-done | bytes 49168 | tf_op jit(solution)/shard_map/reduce_scatter | solution.py:189
  209.9 1.4 add_convert_fusion
  (38 shorter events, 0.2 us)
Async XLA Ops:
  7.2 3.6 %copy-start = (bf16[24,1,1024,64]{2,3,1,0:T(8,128)(2,1)S(1)}, bf16[24,1,1024,64]{2,3,1,0:T(8,128)(2,1)}, u32[]{:S(2)}) copy-start(bf16[24,1,1024,64]{2,3,1,0:T(8,128)(2,1)} %param.28) | copy-start | bytes 9437188
  7.2 3.5 %copy-start.8 = (s32[24]{0:T(128)S(1)}, s32[24]{0:T(128)}, u32[]{:S(2)}) copy-start(s32[24]{0:T(128)} %param.30) | copy-start | bytes 292
  7.2 3.6 %copy-start.7 = (f32[8]{0:T(128)S(1)}, f32[8]{0:T(128)}, u32[]{:S(2)}) copy-start(f32[8]{0:T(128)} %param.27) | copy-start | bytes 100
  7.2 52.1 %all-reduce.5.cloned.1.call-start = ((), (), s32[]{:S(2)}) async-start(), calls=%async_computation.1 | async-start | bytes 196608 | tf_op jit(solution)/shard_map/psum | solution.py:114
  11.3 0.9 copy-start.1
  22.0 2.8 %copy-start.6 = (s32[24,2]{0,1:T(2,128)S(1)}, s32[24,2]{0,1:T(2,128)}, u32[]{:S(2)}) copy-start(s32[24,2]{0,1:T(2,128)} %param.34) | copy-start | bytes 580
  22.0 37.3 %copy-start.2 = (bf16[24,2048]{1,0:T(8,128)(2,1)S(1)}, bf16[24,2048]{1,0:T(8,128)(2,1)}, u32[]{:S(2)}) copy-start(bf16[24,2048]{1,0:T(8,128)(2,1)} %param.21) | copy-start | bytes 294916
  24.8 118.3 %all-reduce.7.cloned.1.call-start = ((), (), s32[]{:S(2)}) async-start(), calls=%async_computation.3 | async-start | bytes 1966080 | tf_op jit(solution)/shard_map/psum | solution.py:156
  60.4 0.7 copy-start.3
  103.0 3.1 %copy-start.4 = (bf16[96,512]{1,0:T(8,128)(2,1)S(1)}, bf16[96,512]{1,0:T(8,128)(2,1)}, u32[]{:S(2)}) copy-start(bf16[96,512]{1,0:T(8,128)(2,1)} %reshape.211) | copy-start | bytes 294916
  103.0 3.1 %copy-start.10 = (bf16[1,512,512]{2,1,0:T(8,128)(2,1)S(1)}, bf16[1,512,512]{2,1,0:T(8,128)(2,1)}, u32[]{:S(2)}) copy-start(bf16[1,512,512]{2,1,0:T(8,128)(2,1)} %param.36) | copy-start | bytes 1572868
  103.0 3.1 %copy-start.11 = (bf16[1,512,512]{2,1,0:T(8,128)(2,1)S(1)}, bf16[1,512,512]{2,1,0:T(8,128)(2,1)}, u32[]{:S(2)}) copy-start(bf16[1,512,512]{2,1,0:T(8,128)(2,1)} %param.35) | copy-start | bytes 1572868
  107.1 102.8 %reduce-scatter.2.cloned.1.call-start = ((), (), s32[]{:S(2)}) async-start(), calls=%async_computation.2 | async-start | bytes 442368 | tf_op jit(solution)/shard_map/reduce_scatter | solution.py:189
  143.0 2.4 %copy-start.12 = (bf16[1,512,512]{2,1,0:T(8,128)(2,1)S(1)}, bf16[1,512,512]{2,1,0:T(8,128)(2,1)}, u32[]{:S(2)}) copy-start(bf16[1,512,512]{2,1,0:T(8,128)(2,1)} %param.37) | copy-start | bytes 1572868
  143.1 2.6 %copy-start.9 = (bf16[1024,512]{1,0:T(8,128)(2,1)S(1)}, bf16[1024,512]{1,0:T(8,128)(2,1)}, u32[]{:S(2)}) copy-start(bf16[1024,512]{1,0:T(8,128)(2,1)} %param.40) | copy-start | bytes 3145732
  145.7 1.5 copy-start.5
Sparse Core Ops, SparseCore 0:
  24.9 34.3 all-reduce.4
  107.2 35.8 all-reduce.6
  147.3 62.5 reduce-scatter.1
where the time goes:
time: 219 us; the launch traced here: 218 us
  waiting for transfers between devices  104 us (47%)
  blocking collectives  59 us (27%)
  matrix products  23.4 us (11%)
  between operations  14 us (6%)
  other arithmetic  8.8 us (4%)
  local copies, waits for them, and re-layouts  8.09 us (4%)
    reduce_scatter x1, waiting for transfers between devices, shards(): lax.psum_scatter(expert_part + mix_gate[:, None] * dense_part, 'ep', scat...  59.1 us
    psum x1, waiting for transfers between devices, shards(): lax.psum(partials[0].astype(jnp.bfloat16), 'tp').astype(jnp.float32)  35.4 us
    all_gather x1, blocking collectives, shards(): every_row = lax.all_gather(h_slice, 'ep', axis=0, tiled=True)  30.8 us
    all_gather x1, blocking collectives, shards(): every_route = lax.all_gather(routes, 'ep', axis=0, tiled=True)  22.3 us
    psum x1, waiting for transfers between devices, shards(): lax.psum(lax.optimization_barrier(partial_value).astype(jnp.float32).asty...  9.9 us
    psum x1, blocking collectives, shards(): lax.psum(partials[3].astype(jnp.bfloat16), 'tp').astype(jnp.float32)  5.9 us
  transfers between devices with their start and end apart: 3, of which 3 were waited for; matrix products, arithmetic and copies ran while one was open for 3% of the time, Pallas kernels for 0%

commit v1 on v0

v1 whole, which is shorter than its diff:
```python
import jax
import jax.numpy as jnp
from jax import lax
from jax.experimental import pallas as pl
from jax.experimental.pallas import tpu as pltpu
from jax.sharding import PartitionSpec as P
import functools

GROUPS = 4
TOP_K = 2


norm_eps = 1e-06
segment_len = 128


def normed(values, gains):
    wide = values.astype(jnp.float32)
    return wide * lax.rsqrt(jnp.mean(wide * wide, axis=-1, keepdims=True) + norm_eps) * gains


def suffix_sums(terms):
    length = terms.shape[-1]
    pieces = length // segment_len
    shaped = terms.reshape(terms.shape[:-1] + (pieces, segment_len))
    inner = lax.iota(jnp.int32, segment_len)
    later_inner = (inner[:, None] > inner[None, :]).astype(jnp.float32)
    within = jnp.einsum("...ij,jk->...ik", shaped, later_inner, precision=lax.Precision.HIGHEST)
    outer = lax.iota(jnp.int32, pieces)
    later_outer = (outer[:, None] > outer[None, :]).astype(jnp.float32)
    carried = jnp.einsum(
        "...i,ij->...j", jnp.sum(shaped, axis=-1), later_outer, precision=lax.Precision.HIGHEST
    )
    return (within + carried[..., None]).reshape(terms.shape)


def stick_read(queries, keys, values, lengths, bias_table):
    scores = jnp.einsum("bkgd,bksd->bkgs", queries, keys, preferred_element_type=jnp.float32)
    scores = scores * queries.shape[-1] ** (-0.5) + bias_table[None, :, :, None]
    positions = lax.iota(jnp.int32, keys.shape[2])
    inside = (positions[None, :] < lengths[:, None])[:, None, None, :]
    fails = jnp.where(inside, jax.nn.log_sigmoid(-scores), 0.0)
    weights = jnp.where(inside, jnp.exp(jax.nn.log_sigmoid(scores) + suffix_sums(fails)), 0.0)
    result = jnp.einsum(
        "bkgs,bksd->bkgd", weights.astype(jnp.bfloat16), values, preferred_element_type=jnp.float32
    )
    return result.astype(jnp.bfloat16).reshape(queries.shape[0], -1)


LANES = 128
MESH = pl.DeviceIdType.MESH


def tail_kernel(
    dims,
    partial_ref, tokens_ref, gain_ref, routes_ref, aux_w_ref,
    dg_hbm, du_hbm, dd_hbm, eg_hbm, eu_hbm, ed_hbm,
    out_ref,
    dg, du, dd, eg, eu, ed,
    route_buf, tp_buf, resid_buf, rows_buf, pick_buf, mask_buf, chosen_buf,
    dsend, drecv, esend, erecv, asend, arecv,
    hid_buf, ehid_buf, dense_buf, eout_buf, fin_send, fin_recv,
    load_sem, rt_s, rt_r, tp_s, tp_r, row_s, row_r, pre_s, pre_r, hid_s, hid_r, fin_s, fin_r,
):
    E, T, S, W, U, F, slots, per_group, fine_count = dims
    ET = E // T
    RB, CB = ET * S, ET * slots
    me_e, me_t = lax.axis_index("ep"), lax.axis_index("tp")

    loads = [
        pltpu.make_async_copy(src, dst, load_sem.at[i])
        for i, (src, dst) in enumerate(
            [(dg_hbm, dg), (du_hbm, du), (eg_hbm, eg), (eu_hbm, eu), (dd_hbm, dd), (ed_hbm, ed)]
        )
    ]
    for load in loads:
        load.start()

    barrier = pltpu.get_barrier_semaphore()

    def greet(d, carry):
        pl.semaphore_signal(
            barrier, inc=1, device_id={"ep": lax.rem(me_e + d, E)}, device_id_type=MESH
        )
        return carry

    lax.fori_loop(1, E, greet, 0)
    for j in range(1, T):
        pl.semaphore_signal(
            barrier, inc=1, device_id={"tp": lax.rem(me_t + j, T)}, device_id_type=MESH
        )
    pl.semaphore_wait(barrier, E - 1 + T - 1)

    def remote(src, dst, send, recv, device):
        return pltpu.make_async_remote_copy(
            src_ref=src, dst_ref=dst, send_sem=send, recv_sem=recv,
            device_id=device, device_id_type=MESH,
        )

    def feature_block(index):
        return pl.ds(pl.multiple_of(index * W, LANES), W)

    tp_copies = []
    for j in range(1, T):
        peer = lax.rem(me_t + j, T)
        tp_copies.append(
            remote(
                partial_ref.at[:, feature_block(peer)], tp_buf.at[j - 1],
                tp_s.at[j - 1], tp_r.at[j - 1], {"tp": peer},
            )
        )
        tp_copies[-1].start()

    def route_copy(d):
        return remote(
            routes_ref, route_buf.at[d], rt_s.at[d], rt_r.at[d], {"ep": lax.rem(me_e + d, E)}
        )

    def row_copy(d):
        return remote(
            rows_buf.at[0], rows_buf.at[d], row_s.at[d], row_r.at[d], {"ep": lax.rem(me_e + d, E)}
        )

    def fin_copy(d):
        return remote(
            fin_send.at[d], fin_recv.at[d], fin_s.at[d], fin_r.at[d],
            {"ep": lax.rem(me_e - d + E, E)},
        )

    def each(first, body):
        def step(d, carry):
            body(d)
            return carry

        lax.fori_loop(first, E, step, 0)

    each(1, lambda d: route_copy(d).start())
    route_buf[0] = routes_ref[...]

    gain = gain_ref[:, feature_block(me_t)]
    total = tokens_ref[:, feature_block(me_t)].astype(jnp.float32)
    total = total + partial_ref[:, feature_block(me_t)].astype(jnp.float32)
    for j in range(1, T):
        tp_copies[j - 1].wait_recv()
        total = total + tp_buf[j - 1].astype(jnp.float32)
    resid_buf[...] = total
    rows_buf[0] = (total * gain).astype(jnp.bfloat16)
    each(1, lambda d: row_copy(d).start())

    each(1, lambda d: route_copy(d).wait_recv())
    own = me_e.astype(jnp.float32)
    before = (
        lax.broadcasted_iota(jnp.int32, (LANES, LANES), 0)
        < lax.broadcasted_iota(jnp.int32, (LANES, LANES), 1)
    ).astype(jnp.float32).astype(jnp.bfloat16)
    slot_iota = lax.broadcasted_iota(jnp.int32, (slots, LANES), 0).astype(jnp.float32)
    lane_iota = lax.broadcasted_iota(jnp.int32, (slots, LANES), 1).astype(jnp.float32)

    def pick(d):
        named = route_buf[d]
        hits = jnp.where(named == own, 1.0, 0.0)
        ranks = jnp.dot(hits.astype(jnp.bfloat16), before, preferred_element_type=jnp.float32)
        rank = jnp.sum(ranks, axis=0, keepdims=True)
        hit = jnp.sum(hits, axis=0, keepdims=True)
        picks = jnp.where(slot_iota == rank, 1.0, 0.0) * hit
        pick_buf[d] = picks
        mask = jnp.zeros((slots, LANES), jnp.float32)
        for i in range(TOP_K):
            chosen = jnp.sum(picks * named[i : i + 1, :], axis=1, keepdims=True)
            mask = jnp.where(lane_iota == chosen + float(GROUPS), 1.0, mask)
        mask_buf[d] = mask

    each(0, pick)

    def gather(d):
        chosen_buf[d] = jnp.dot(
            pick_buf[d][:, :S].astype(jnp.bfloat16), rows_buf[d],
            preferred_element_type=jnp.float32,
        )

    gather(0)

    def gather_arrived(d):
        row_copy(d).wait_recv()
        gather(d)

    each(1, gather_arrived)
    for load in loads[:4]:
        load.wait()

    inverse = 1.0 / gain
    aux_w = aux_w_ref[me_t]

    def dot(a, b):
        return jnp.dot(a, b, preferred_element_type=jnp.float32)

    def partials(owner):
        rows = rows_buf[pl.ds(owner * ET, ET)].astype(jnp.float32).reshape(RB, W)
        picked = chosen_buf[pl.ds(owner * ET, ET)].reshape(CB, W)
        both = jnp.concatenate([rows, picked], axis=0)
        scaled = both * inverse
        squares = jnp.sum(scaled * scaled, axis=1, keepdims=True)
        rows, picked = rows.astype(jnp.bfloat16), picked.astype(jnp.bfloat16)
        lanes = lax.broadcasted_iota(jnp.int32, (RB + CB, LANES), 1)
        aux = dot(both.astype(jnp.bfloat16), aux_w) + jnp.where(lanes == LANES - 1, squares, 0.0)
        return rows, picked, aux

    pre_copies = []
    for j in range(1, T):
        owner = lax.rem(me_t + j, T)
        rows, picked, aux = partials(owner)
        dsend[j - 1, :, :U] = dot(rows, dg[...]).astype(jnp.bfloat16)
        dsend[j - 1, :, U:] = dot(rows, du[...]).astype(jnp.bfloat16)
        esend[j - 1, :, :F] = dot(picked, eg[...]).astype(jnp.bfloat16)
        esend[j - 1, :, F:] = dot(picked, eu[...]).astype(jnp.bfloat16)
        asend[j - 1] = aux
        for k, (src, dst) in enumerate([(dsend, drecv), (esend, erecv), (asend, arecv)]):
            copy = remote(
                src.at[j - 1], dst.at[j - 1], pre_s.at[j - 1, k], pre_r.at[j - 1, k], {"tp": owner}
            )
            copy.start()
            pre_copies.append(copy)
    rows, picked, aux = partials(me_t)
    gate, up = dot(rows, dg[...]), dot(rows, du[...])
    egate, eup = dot(picked, eg[...]), dot(picked, eu[...])
    for copy in pre_copies:
        copy.wait_recv()
    for j in range(T - 1):
        aux = aux + arecv[j]
        gate = gate + drecv[j, :, :U].astype(jnp.float32)
        up = up + drecv[j, :, U:].astype(jnp.float32)
        egate = egate + erecv[j, :, :F].astype(jnp.float32)
        eup = eup + erecv[j, :, F:].astype(jnp.float32)
    scale = lax.rsqrt(aux[:, LANES - 1 :] / (T * W) + norm_eps)
    logits = aux * scale
    mix = GROUPS + fine_count
    mix_gate = jax.nn.sigmoid(logits[:RB, mix : mix + 1] + logits[:RB, mix + 1 : mix + 2])
    dense_scale, slot_scale = scale[:RB], scale[RB:]
    gate, up = gate * dense_scale, up * dense_scale
    hid_buf[me_t] = (jax.nn.silu(gate) * up * mix_gate).astype(jnp.bfloat16)

    slot_logits = logits[RB:]
    lanes = lax.broadcasted_iota(jnp.int32, (CB, LANES), 1)

    def at_lane(lane):
        return jnp.sum(jnp.where(lanes == lane, slot_logits, 0.0), axis=1, keepdims=True)

    own_group, own_fine = at_lane(me_e // per_group), at_lane(me_e + GROUPS)
    named = mask_buf[pl.ds(me_t * ET, ET)].reshape(CB, LANES)

    def share(inside, own_logit):
        terms = jnp.exp(jnp.where(inside, slot_logits - own_logit, -jnp.inf))
        return 1.0 / jnp.sum(terms, axis=1, keepdims=True)

    shares = share(lanes < GROUPS, own_group) * share(
        (named > 0.0) | (lanes == me_e + GROUPS), own_fine
    )
    egate, eup = egate * slot_scale, eup * slot_scale
    ehid_buf[me_t] = (jax.nn.silu(egate) * eup * shares).astype(jnp.bfloat16)

    hid_copies = []
    for j in range(1, T):
        for k, buf in enumerate([hid_buf, ehid_buf]):
            copy = remote(
                buf.at[me_t], buf.at[me_t], hid_s.at[j - 1, k], hid_r.at[j - 1, k],
                {"tp": lax.rem(me_t + j, T)},
            )
            copy.start()
            hid_copies.append(copy)
    for load in loads[4:]:
        load.wait()
    for copy in hid_copies:
        copy.wait_recv()

    dense_buf[...] = dot(hid_buf[...].reshape(E * S, U), dd[...]).reshape(E, S, W)
    eout_buf[...] = dot(ehid_buf[...].reshape(E * slots, F), ed[...]).reshape(E, slots, W)

    def output_of(d):
        back = pick_buf[d].T[:S].astype(jnp.bfloat16)
        return dense_buf[d] + dot(back, eout_buf[d].astype(jnp.bfloat16))

    def finish(d):
        fin_send[d] = output_of(d).astype(jnp.bfloat16)
        fin_copy(d).start()

    each(1, finish)
    resid_buf[...] += output_of(0)

    def collect(d):
        fin_copy(d).wait_recv()
        resid_buf[...] += fin_recv[d].astype(jnp.float32)

    each(1, collect)
    out_ref[...] = resid_buf[...].astype(jnp.bfloat16)

    for copy in tp_copies + pre_copies + hid_copies:
        copy.wait_send()
    each(1, lambda d: route_copy(d).wait_send())
    each(1, lambda d: row_copy(d).wait_send())
    each(1, lambda d: fin_copy(d).wait_send())


def tail(partial, tokens, gain, routes, w_group, w_fine, w_mix, dg, du, dd, eg, eu, ed):
    E, T = lax.axis_size("ep"), lax.axis_size("tp")
    S, D = tokens.shape
    W, U = dg.shape
    F = eg.shape[1]
    per_group = E // GROUPS
    capacity = max(2, (S + per_group - 1) // per_group)
    slots = (capacity + 7) // 8 * 8
    ET = E // T
    RB, CB = ET * S, ET * slots
    high = lax.reduce_precision(w_mix, 8, 7)
    aux_w = jnp.concatenate(
        [w_group, w_fine, high.astype(jnp.bfloat16)[:, None],
         (w_mix - high).astype(jnp.bfloat16)[:, None]], axis=1,
    )
    aux_w = jnp.pad(aux_w, ((0, 0), (0, LANES - aux_w.shape[1]))).reshape(T, W, LANES)
    route_rows = jnp.pad(
        routes.T.astype(jnp.float32), ((0, 8 - TOP_K), (0, LANES - S)), constant_values=-1.0
    )
    bf16, f32 = jnp.bfloat16, jnp.float32
    vmem = pl.BlockSpec(memory_space=pltpu.VMEM)
    anywhere = pl.BlockSpec(memory_space=pl.ANY)
    dma = pltpu.SemaphoreType.DMA
    dims = (E, T, S, W, U, F, slots, per_group, w_fine.shape[1])
    return pl.pallas_call(
        functools.partial(tail_kernel, dims),
        out_shape=jax.ShapeDtypeStruct((S, W), bf16),
        in_specs=[vmem] * 5 + [anywhere] * 6,
        out_specs=vmem,
        scratch_shapes=[
            pltpu.VMEM((W, U), bf16), pltpu.VMEM((W, U), bf16), pltpu.VMEM((U, W), bf16),
            pltpu.VMEM((W, F), bf16), pltpu.VMEM((W, F), bf16), pltpu.VMEM((F, W), bf16),
            pltpu.VMEM((E, 8, LANES), f32),
            pltpu.VMEM((T - 1, S, W), bf16),
            pltpu.VMEM((S, W), f32),
            pltpu.VMEM((E, S, W), bf16),
            pltpu.VMEM((E, slots, LANES), f32),
            pltpu.VMEM((E, slots, LANES), f32),
            pltpu.VMEM((E, slots, W), f32),
            pltpu.VMEM((T - 1, RB, 2 * U), bf16), pltpu.VMEM((T - 1, RB, 2 * U), bf16),
            pltpu.VMEM((T - 1, CB, 2 * F), bf16), pltpu.VMEM((T - 1, CB, 2 * F), bf16),
            pltpu.VMEM((T - 1, RB + CB, LANES), f32), pltpu.VMEM((T - 1, RB + CB, LANES), f32),
            pltpu.VMEM((T, RB, U), bf16), pltpu.VMEM((T, CB, F), bf16),
            pltpu.VMEM((E, S, W), f32), pltpu.VMEM((E, slots, W), f32),
            pltpu.VMEM((E, S, W), bf16), pltpu.VMEM((E, S, W), bf16),
            dma((6,)), dma((E,)), dma((E,)), dma((T - 1,)), dma((T - 1,)), dma((E,)), dma((E,)),
            dma((T - 1, 3)), dma((T - 1, 3)), dma((T - 1, 2)), dma((T - 1, 2)),
            dma((E,)), dma((E,)),
        ],
        compiler_params=pltpu.CompilerParams(
            collective_id=0, has_side_effects=True, vmem_limit_bytes=48 * 1024 * 1024
        ),
        name="tail",
    )(partial, tokens, gain[None, :], route_rows, aux_w, dg, du, dd, eg, eu, ed)


def shards(
    tokens,
    norm_attn,
    w_query,
    w_key,
    w_value,
    w_out,
    head_bias,
    key_cache,
    value_cache,
    lengths,
    norm_ffn,
    w_group,
    w_fine,
    routes,
    e_gate,
    e_up,
    e_down,
    d_gate,
    d_up,
    d_down,
    w_mix,
):
    seq_count = tokens.shape[0]
    kv_local = key_cache.shape[1]
    head_dim = key_cache.shape[3]
    h_first = normed(tokens, norm_attn).astype(jnp.bfloat16)
    queries = jnp.dot(h_first, w_query, preferred_element_type=jnp.float32).astype(jnp.bfloat16)
    new_keys = jnp.dot(h_first, w_key, preferred_element_type=jnp.float32).astype(jnp.bfloat16)
    new_values = jnp.dot(h_first, w_value, preferred_element_type=jnp.float32).astype(jnp.bfloat16)
    grouped = queries.reshape(seq_count, kv_local, -1, head_dim)
    heads_out = stick_read(
        grouped, key_cache, value_cache, lengths, head_bias.reshape(kv_local, -1)
    )
    partial_value = jnp.dot(heads_out, w_out, preferred_element_type=jnp.float32).astype(
        jnp.bfloat16
    )
    mixed = tail(
        partial_value, tokens, norm_ffn, routes, w_group, w_fine, w_mix,
        d_gate, d_up, d_down, e_gate[0], e_up[0], e_down[0],
    )
    return (
        mixed,
        new_keys.reshape(seq_count, kv_local, head_dim),
        new_values.reshape(seq_count, kv_local, head_dim),
    )


def solution(mesh):
    placed = (
        P("ep", None),
        P(),
        P(None, "tp"),
        P(None, "tp"),
        P(None, "tp"),
        P("tp", None),
        P("tp"),
        P("ep", "tp", None, None),
        P("ep", "tp", None, None),
        P("ep"),
        P(),
        P(),
        P(),
        P("ep", None),
        P("ep", "tp", None),
        P("ep", "tp", None),
        P("ep", None, "tp"),
        P("tp", "ep"),
        P("tp", "ep"),
        P("ep", "tp"),
        P(),
    )
    return jax.shard_map(
        shards,
        mesh=mesh,
        in_specs=placed,
        out_specs=(P("ep", "tp"), P("ep", "tp", None), P("ep", "tp", None)),
        check_vma=False,
    )
```

time: 219 us -> 74.5 us (0.34)
  waiting for transfers between devices: 104 us -> 0 us
  blocking collectives: 59 us -> 0 us
  Pallas kernels: 0 us -> 44.3 us
  between operations: 14 us -> 0.85 us
  matrix products: 23.4 us -> 13 us
  other arithmetic: 8.8 us -> 2.76 us
  local copies, waits for them, and re-layouts: 8.09 us -> 13.1 us
    reduce_scatter x1 -> x0, waiting for transfers between devices: 59.1 us -> none  [shards(): lax.psum_scatter(expert_part + mix_gate[:, None] * dense_part, 'ep', scat...]
    all_gather x2 -> x0, blocking collectives: 53.1 us -> none  [the longest x1 30.8 us: shards(): every_row = lax.all_gather(h_slice, 'ep', axis=0, tiled=True)]
    psum x2 -> x0, waiting for transfers between devices: 45.3 us -> none  [the longest x1 35.4 us: shards(): lax.psum(partials[0].astype(jnp.bfloat16), 'tp').astype(jnp.float32)]
    pallas_call x0 -> x1, Pallas kernels: none -> 44.3 us  [tail(): pl.pallas_call(functools.partial(tail_kernel, dims), out_shape=jax.ShapeD...]
    dot_general x9 -> x0, matrix products: 8.51 us -> none  [the longest x1 3.1 us: shards(): jnp.dot(every_row, dense_in, preferred_element_type=jnp.float32)]
    unnamed x27 -> x38, local copies, waits for them, and re-layouts: 1.66 us -> 9.31 us
    psum x1 -> x0, blocking collectives: 5.9 us -> none  [shards(): lax.psum(partials[3].astype(jnp.bfloat16), 'tp').astype(jnp.float32)]
    convert_element_type x6 -> x2, other arithmetic: 3.9 us -> 0.01 us  [the longest x1 0.01 us: tail(): high.astype(jnp.bfloat16)[:, None]]
  transfers between devices with their start and end apart: 3 -> 0, of which waited for: 3 -> 0; matrix products, arithmetic and copies ran while one was open for 3% -> 0% of each run, Pallas kernels for 0% -> 0%
where the time goes in v1:
time: 74.5 us; the launch traced here: 74 us
  Pallas kernels  44.3 us (59%)
  local copies, waits for them, and re-layouts  13.1 us (18%)
  matrix products  13 us (17%)
  other arithmetic  2.76 us (4%)
  between operations  0.85 us (1%)
    pallas_call x1, Pallas kernels, tail(): pl.pallas_call(functools.partial(tail_kernel, dims), out_shape=jax.ShapeD...  44.3 us
    unnamed x38, local copies, waits for them, and re-layouts  9.31 us
    dot_general x1, matrix products, stick_read(): jnp.einsum('bkgs,bksd->bkgd', weights.astype(jnp.bfloat16), values, prefe...  3.32 us
    dot_general x1, matrix products, suffix_sums(): jnp.einsum('...ij,jk->...ik', shaped, later_inner, precision=lax.Precisio...  2.63 us
    reshape x1, local copies, waits for them, and re-layouts, suffix_sums(): return (within + carried[..., None]).reshape(terms.shape)  2.13 us
    dot_general x1, matrix products, shards(): jnp.dot(h_first, w_query, preferred_element_type=jnp.float32)  2.09 us
    dot_general x1, matrix products, shards(): jnp.dot(heads_out, w_out, preferred_element_type=jnp.float32)  1.98 us

profile of v1, /device:TPU:0, one launch (start us, length us, event | category | flops | bytes accessed | tf_op | source)
XLA Modules:
  0.0 74.0 jit_solution(4274270423972925602)
XLA Ops:
  0.6 0.0 copy-start
  0.6 1.2 %fusion.27 = f32[24]{0:T(128)S(1)} fusion(bf16[24,2048]{1,0:T(8,128)(2,1)} %tokens_ref.1), kind=kLoop, calls=%fused_computation.29 | loop fusion | flops 147432 | bytes 98400 | tf_op jit(solution)/shard_map/reduce_sum | solution.py:19
  1.8 0.0 copy-start.15
  1.8 2.1 %convolution_convert_fusion.1 = bf16[24,512]{1,0:T(8,128)(2,1)S(1)} fusion(bf16[2048,512]{1,0:T(8,128)(2,1)} %param.23, bf16[24,2048]{1,0:T(8,128)(2,1)} %tokens_ref.1, f32[2048]{0:T(1024)} %param.22, f32[24]{0:T(128)S(1)} %add_rsqrt_fusion), kind=kOutput, calls=%fused_computation.11 | convolution fusion | flops 50540544 | bytes 2228320 | tf_op jit(solution)/shard_map/dot_general | solution.py:386
  3.9 0.1 reshape.114
  4.0 0.0 copy-done
  4.1 1.2 %fusion.7 = f32[24,8,1024]{2,1,0:T(8,128)S(1)} fusion(bf16[24,8,64]{2,1,0:T(8,128)(2,1)S(1)} %reshape.114, bf16[24,1,1024,64]{2,3,1,0:T(8,128)(2,1)S(1)} %copy-done, f32[8]{0:T(128)} %param.27), kind=kOutput, calls=%fused_computation.9 | convolution fusion | flops 25559040 | bytes 3956768 | tf_op jit(solution)/shard_map/bkgd,bksd->bkgs/dot_general | solution.py:38
  5.2 0.0 copy-done.15
  5.2 0.0 copy-start.9
  5.3 0.1 iota_compare_fusion
  5.3 0.8 %copy-done.9 = f32[24,8,1024]{2,1,0:T(8,128)} copy-done((f32[24,8,1024]{2,1,0:T(8,128)}, f32[24,8,1024]{2,1,0:T(8,128)S(1)}, u32[]{:S(2)}) %copy-start.9) | copy-done | bytes 786456
  6.2 1.4 %fusion.40 = (f32[24,8,8]{1,2,0:T(8,128)S(1)}, f32[24,8,8,128]{3,1,2,0:T(8,128)}) fusion(f32[24,8,1024]{2,1,0:T(8,128)S(1)} %fusion.7, pred[24,1024]{1,0:T(8,128)(4,1)S(1)} %iota_compare_fusion), kind=kLoop, calls=%fused_computation.45 | loop fusion | flops 1767936 | bytes 1603584 | tf_op jit(solution)/shard_map/reduce_sum | solution.py:32
  7.6 0.1 copy.28
  7.7 0.1 fusion.34
  7.8 0.1 copy.29
  7.9 2.6 %convolution_add_fusion = f32[24,8,8,128]{3,2,1,0:T(8,128)} fusion(f32[24,8,8,128]{3,1,2,0:T(8,128)} %get-tuple-element.4, f32[24,8,8]{2,1,0:T(8,128)S(1)} %copy.29), kind=kOutput, calls=%fused_computation.7 | convolution fusion | flops 302202880 | bytes 1579008 | tf_op jit(solution)/shard_map/...ij,jk->...ik/dot_general | solution.py:28
  10.6 2.1 %reshape.117 = f32[24,8,1024]{2,1,0:T(8,128)} reshape(f32[24,8,8,128]{3,2,1,0:T(8,128)} %convolution_add_fusion) | data formatting | bytes 1572864 | tf_op jit(solution)/shard_map/reshape | solution.py:34
  12.7 0.0 copy-start.13
  12.7 0.0 copy-start.10
  12.7 0.0 copy-start.11
  12.7 3.3 %fusion.10 = bf16[24,8,64]{2,1,0:T(8,128)(2,1)S(1)} fusion(bf16[24,1,1024,64]{2,3,1,0:T(8,128)(2,1)} %param.29, f32[24,8,1024]{2,1,0:T(8,128)} %reshape.117, f32[24,8,1024]{2,1,0:T(8,128)} %copy-done.9, pred[24,1024]{1,0:T(8,128)(4,1)S(1)} %iota_compare_fusion), kind=kOutput, calls=%fused_computation.10 | convolution fusion | flops 27340800 | bytes 4767744 | tf_op jit(solution)/shard_map/bkgs,bksd->bkgd/dot_general | solution.py:44
  16.0 0.0 copy-start.14
  16.0 0.0 copy-start.4
  16.0 0.0 copy-start.8
  16.1 0.1 reshape.119
  16.2 2.0 %convolution_convert_fusion.partial_ref = bf16[24,2048]{1,0:T(8,128)(2,1)S(1)} fusion(bf16[24,512]{1,0:T(8,128)(2,1)S(1)} %reshape.119, bf16[512,2048]{1,0:T(8,128)(2,1)} %param.26), kind=kOutput, calls=%fused_computation.6 | convolution fusion | flops 50380800 | bytes 2220032 | tf_op jit(solution)/shard_map/dot_general | solution.py:393
  18.1 0.0 copy-done.13
  18.2 0.0 copy-done.10
  18.2 0.0 copy-done.11
  18.3 1.0 %copy.32 = bf16[2048,14]{1,0:T(8,128)(2,1)} copy(bf16[2048,14]{0,1:T(8,128)(2,1)S(1)} %pad_maximum_fusion) | data formatting | bytes 114688
  19.3 0.0 copy-start.12
  19.3 0.0 copy-start.16
  19.3 0.0 copy-start.17
  19.3 1.2 %pad.9.clone = bf16[2048,128]{1,0:T(8,128)(2,1)S(1)} pad(bf16[2048,14]{1,0:T(8,128)(2,1)} %copy.32, bf16[]{:T(256)} %constant.17.clone.1), padding=0_0x0_114 | pad | bytes 581634 | tf_op jit(solution)/shard_map/jit(_pad)/pad | solution.py:318
  20.5 0.0 copy-done.14
  20.6 0.0 copy-done.4
  20.6 0.0 copy-done.8
  20.6 0.0 copy-start.1
  20.6 1.2 %copy-done.1 = bf16[512,1024]{1,0:T(8,128)(2,1)S(1)} copy-done((bf16[512,1024]{1,0:T(8,128)(2,1)S(1)}, bf16[512,1024]{1,0:T(8,128)(2,1)}, u32[]{:S(2)}) %copy-start.1) | copy-done | bytes 1048600
  21.8 0.0 copy-start.2
  21.8 1.2 %copy-done.2 = bf16[512,1024]{1,0:T(8,128)(2,1)S(1)} copy-done((bf16[512,1024]{1,0:T(8,128)(2,1)S(1)}, bf16[512,1024]{1,0:T(8,128)(2,1)}, u32[]{:S(2)}) %copy-start.2) | copy-done | bytes 1048600
  23.0 0.0 copy-start.3
  23.0 1.2 %copy-done.3 = bf16[1024,512]{1,0:T(8,128)(2,1)S(1)} copy-done((bf16[1024,512]{1,0:T(8,128)(2,1)S(1)}, bf16[1024,512]{1,0:T(8,128)(2,1)}, u32[]{:S(2)}) %copy-start.3) | copy-done | bytes 1048600
  24.3 0.0 copy-start.5
  24.3 1.0 %copy-done.5 = bf16[1,512,512]{2,1,0:T(8,128)(2,1)S(1)} copy-done((bf16[1,512,512]{2,1,0:T(8,128)(2,1)S(1)}, bf16[1,512,512]{2,1,0:T(8,128)(2,1)}, u32[]{:S(2)}) %copy-start.5) | copy-done | bytes 524312
  25.3 0.0 copy-start.6
  25.3 1.0 %copy-done.6 = bf16[1,512,512]{2,1,0:T(8,128)(2,1)S(1)} copy-done((bf16[1,512,512]{2,1,0:T(8,128)(2,1)S(1)}, bf16[1,512,512]{2,1,0:T(8,128)(2,1)}, u32[]{:S(2)}) %copy-start.6) | copy-done | bytes 524312
  26.3 0.0 copy-start.7
  26.4 1.0 %copy-done.7 = bf16[1,512,512]{2,1,0:T(8,128)(2,1)S(1)} copy-done((bf16[1,512,512]{2,1,0:T(8,128)(2,1)S(1)}, bf16[1,512,512]{2,1,0:T(8,128)(2,1)}, u32[]{:S(2)}) %copy-start.7) | copy-done | bytes 524312
  27.4 44.3 %tail.1 = bf16[24,512]{1,0:T(8,128)(2,1)S(1)} custom-call(bf16[24,2048]{1,0:T(8,128)(2,1)S(1)} %convolution_convert_fusion.partial_ref, bf16[24,2048]{1,0:T(8,128)(2,1)S(1)} %copy-done.4, f32[1,2048]{1,0:T(1,128)S(1)} %bitcast.47, f32[8,128]{1,0:T(8,128)S(1)} %pad.8.routes_ref, bf16[4,512,128]{2,1,0:T(8,128)(2,1)S(1)} %bitcast.43, ...), custom_call_target="tpu_custom_call" | custom-call | tf_op jit(solution)/shard_map/tail/pallas_call | solution.py:327
  71.7 0.0 copy-done.12
  71.7 0.0 copy-done.16
  71.7 0.9 %fusion.13 = bf16[24,1,64]{2,0,1:T(8,128)(2,1)} fusion(bf16[2048,64]{0,1:T(8,128)(2,1)S(1)} %copy-done.16, bf16[24,2048]{1,0:T(8,128)(2,1)S(1)} %copy-done.4, f32[2048]{0:T(1024)S(1)} %copy-done.12, f32[24]{0:T(128)S(1)} %add_rsqrt_fusion), kind=kOutput, calls=%fused_computation.14 | convolution fusion | flops 6489600 | bytes 371808 | tf_op jit(solution)/shard_map/dot_general | solution.py:387
  72.5 0.0 copy-done.17
  72.5 0.8 %fusion.14 = bf16[24,1,64]{2,0,1:T(8,128)(2,1)} fusion(bf16[2048,64]{0,1:T(8,128)(2,1)S(1)} %copy-done.17, bf16[24,2048]{1,0:T(8,128)(2,1)S(1)} %copy-done.4, f32[2048]{0:T(1024)S(1)} %copy-done.12, f32[24]{0:T(128)S(1)} %add_rsqrt_fusion), kind=kOutput, calls=%fused_computation.15 | convolution fusion | flops 6489600 | bytes 371808 | tf_op jit(solution)/shard_map/dot_general | solution.py:388
  73.4 0.6 copy.36
  (7 shorter events, 0.1 us)
Async XLA Ops:
  0.6 3.4 %copy-start = (bf16[24,1,1024,64]{2,3,1,0:T(8,128)(2,1)S(1)}, bf16[24,1,1024,64]{2,3,1,0:T(8,128)(2,1)}, u32[]{:S(2)}) copy-start(bf16[24,1,1024,64]{2,3,1,0:T(8,128)(2,1)} %param.28) | copy-start | bytes 9437188
  1.8 3.4 %copy-start.15 = (s32[24]{0:T(128)S(1)}, s32[24]{0:T(128)}, u32[]{:S(2)}) copy-start(s32[24]{0:T(128)} %param.30) | copy-start | bytes 292
  5.2 0.9 %copy-start.9 = (f32[24,8,1024]{2,1,0:T(8,128)}, f32[24,8,1024]{2,1,0:T(8,128)S(1)}, u32[]{:S(2)}) copy-start(f32[24,8,1024]{2,1,0:T(8,128)S(1)} %fusion.7) | copy-start | bytes 2359300
  12.7 5.4 %copy-start.13 = (f32[2048]{0:T(1024)S(1)}, f32[2048]{0:T(1024)}, u32[]{:S(2)}) copy-start(f32[2048]{0:T(1024)} %param.41) | copy-start | bytes 24580
  12.7 5.5 %copy-start.10 = (bf16[2048,8]{0,1:T(8,128)(2,1)S(1)}, bf16[2048,8]{0,1:T(8,128)(2,1)}, u32[]{:S(2)}) copy-start(bf16[2048,8]{0,1:T(8,128)(2,1)} %param.33) | copy-start | bytes 98308
  12.7 5.5 %copy-start.11 = (bf16[2048,4]{0,1:T(4,128)(2,1)S(1)}, bf16[2048,4]{0,1:T(4,128)(2,1)}, u32[]{:S(2)}) copy-start(bf16[2048,4]{0,1:T(4,128)(2,1)} %param.32) | copy-start | bytes 49156
  16.0 4.5 %copy-start.14 = (s32[24,2]{0,1:T(2,128)S(1)}, s32[24,2]{0,1:T(2,128)}, u32[]{:S(2)}) copy-start(s32[24,2]{0,1:T(2,128)} %param.34) | copy-start | bytes 580
  16.0 4.5 %copy-start.4 = (bf16[24,2048]{1,0:T(8,128)(2,1)S(1)}, bf16[24,2048]{1,0:T(8,128)(2,1)}, u32[]{:S(2)}) copy-start(bf16[24,2048]{1,0:T(8,128)(2,1)} %tokens_ref.1) | copy-start | bytes 294916
  16.0 4.5 %copy-start.8 = (f32[2048]{0:T(1024)S(1)}, f32[2048]{0:T(1024)}, u32[]{:S(2)}) copy-start(f32[2048]{0:T(1024)} %param.31) | copy-start | bytes 24580
  19.3 52.4 %copy-start.12 = (f32[2048]{0:T(1024)S(1)}, f32[2048]{0:T(1024)}, u32[]{:S(2)}) copy-start(f32[2048]{0:T(1024)} %param.22) | copy-start | bytes 24580
  19.3 52.4 %copy-start.16 = (bf16[2048,64]{0,1:T(8,128)(2,1)S(1)}, bf16[2048,64]{0,1:T(8,128)(2,1)}, u32[]{:S(2)}) copy-start(bf16[2048,64]{0,1:T(8,128)(2,1)} %param.24) | copy-start | bytes 786436
  19.3 53.2 %copy-start.17 = (bf16[2048,64]{0,1:T(8,128)(2,1)S(1)}, bf16[2048,64]{0,1:T(8,128)(2,1)}, u32[]{:S(2)}) copy-start(bf16[2048,64]{0,1:T(8,128)(2,1)} %param.25) | copy-start | bytes 786436
  20.6 1.2 %copy-start.1 = (bf16[512,1024]{1,0:T(8,128)(2,1)S(1)}, bf16[512,1024]{1,0:T(8,128)(2,1)}, u32[]{:S(2)}) copy-start(bf16[512,1024]{1,0:T(8,128)(2,1)} %dg_hbm.1) | copy-start | bytes 3145732
  21.8 1.2 %copy-start.2 = (bf16[512,1024]{1,0:T(8,128)(2,1)S(1)}, bf16[512,1024]{1,0:T(8,128)(2,1)}, u32[]{:S(2)}) copy-start(bf16[512,1024]{1,0:T(8,128)(2,1)} %du_hbm.1) | copy-start | bytes 3145732
  23.0 1.2 %copy-start.3 = (bf16[1024,512]{1,0:T(8,128)(2,1)S(1)}, bf16[1024,512]{1,0:T(8,128)(2,1)}, u32[]{:S(2)}) copy-start(bf16[1024,512]{1,0:T(8,128)(2,1)} %dd_hbm.1) | copy-start | bytes 3145732
  24.3 1.0 %copy-start.5 = (bf16[1,512,512]{2,1,0:T(8,128)(2,1)S(1)}, bf16[1,512,512]{2,1,0:T(8,128)(2,1)}, u32[]{:S(2)}) copy-start(bf16[1,512,512]{2,1,0:T(8,128)(2,1)} %param.35) | copy-start | bytes 1572868
  25.3 1.0 %copy-start.6 = (bf16[1,512,512]{2,1,0:T(8,128)(2,1)S(1)}, bf16[1,512,512]{2,1,0:T(8,128)(2,1)}, u32[]{:S(2)}) copy-start(bf16[1,512,512]{2,1,0:T(8,128)(2,1)} %param.36) | copy-start | bytes 1572868
  26.3 1.0 %copy-start.7 = (bf16[1,512,512]{2,1,0:T(8,128)(2,1)S(1)}, bf16[1,512,512]{2,1,0:T(8,128)(2,1)}, u32[]{:S(2)}) copy-start(bf16[1,512,512]{2,1,0:T(8,128)(2,1)} %param.37) | copy-start | bytes 1572868

commit v2 on v1

v2 whole, which is shorter than its diff:
```python
import jax
import jax.numpy as jnp
from jax import lax
from jax.experimental import pallas as pl
from jax.experimental.pallas import tpu as pltpu
from jax.sharding import PartitionSpec as P
import functools

GROUPS = 4
TOP_K = 2


norm_eps = 1e-06


def normed(values, gains):
    wide = values.astype(jnp.float32)
    return wide * lax.rsqrt(jnp.mean(wide * wide, axis=-1, keepdims=True) + norm_eps) * gains


def stick_kernel(batch, heads, lengths_ref, bias_ref, q_ref, k_ref, v_ref, out_ref):
    step = pl.program_id(0)
    head_dim, length = k_ref.shape[1:]
    pieces = length // LANES
    rows = batch * heads
    head = lax.broadcasted_iota(jnp.int32, (heads, length), 0)
    position = lax.broadcasted_iota(jnp.int32, (heads, length), 1)
    bias = jnp.zeros((heads, length), jnp.float32)
    for h in range(heads):
        bias = jnp.where(head == h, bias_ref[h], bias)
    parts, insides = [], []
    for i in range(batch):
        product = jnp.dot(q_ref[i], k_ref[i], preferred_element_type=jnp.float32)
        parts.append(product * head_dim ** (-0.5) + bias)
        insides.append((position < lengths_ref[step * batch + i]).astype(jnp.float32))
    scores = jnp.concatenate(parts, axis=0)
    inside = jnp.concatenate(insides, axis=0) > 0.0
    log_fail = -(jnp.maximum(scores, 0.0) + jnp.log1p(jnp.exp(-jnp.abs(scores))))
    fails = jnp.where(inside, log_fail, 0.0)
    stacked = jnp.concatenate(
        [fails[:, p * LANES : (p + 1) * LANES] for p in range(pieces)], axis=0
    )
    later = (
        lax.broadcasted_iota(jnp.int32, (LANES, LANES), 0)
        > lax.broadcasted_iota(jnp.int32, (LANES, LANES), 1)
    ).astype(jnp.float32).astype(jnp.bfloat16)
    within, left = jnp.zeros_like(stacked), stacked
    for _ in range(3):
        part = left.astype(jnp.bfloat16)
        left = left - part.astype(jnp.float32)
        within = within + jnp.dot(part, later, preferred_element_type=jnp.float32)
    totals = jnp.sum(stacked, axis=1, keepdims=True)
    carry, sums = jnp.zeros((rows, 1), jnp.float32), [None] * pieces
    for p in reversed(range(pieces)):
        sums[p] = within[p * rows : (p + 1) * rows] + carry
        carry = carry + totals[p * rows : (p + 1) * rows]
    suffix = jnp.concatenate(sums, axis=1)
    stick = jnp.where(inside, jnp.exp(scores + log_fail + suffix), 0.0)
    for i in range(batch):
        out_ref[i] = lax.dot_general(
            stick[i * heads : (i + 1) * heads].astype(jnp.bfloat16), v_ref[i],
            (((1,), (1,)), ((), ())), preferred_element_type=jnp.float32,
        ).astype(jnp.bfloat16)


def stick_read(queries, keys, values, lengths, bias):
    count, heads, head_dim = queries.shape
    length = keys.shape[2]
    batch = next(b for b in (4, 3, 2, 1) if count % b == 0)
    smem = pl.BlockSpec(memory_space=pltpu.SMEM)
    cache = pl.BlockSpec((batch, head_dim, length), lambda i: (i, 0, 0))
    small = pl.BlockSpec((batch, heads, head_dim), lambda i: (i, 0, 0))
    return pl.pallas_call(
        functools.partial(stick_kernel, batch, heads),
        grid=(count // batch,),
        out_shape=jax.ShapeDtypeStruct(queries.shape, jnp.bfloat16),
        in_specs=[smem, smem, small, cache, cache],
        out_specs=small,
        cost_estimate=pl.CostEstimate(
            flops=4 * count * heads * head_dim * length,
            bytes_accessed=4 * count * head_dim * length,
            transcendentals=3 * count * heads * length,
        ),
        name="stick",
    )(lengths, bias, queries, keys, values).reshape(count, -1)


LANES = 128
MESH = pl.DeviceIdType.MESH


def tail_kernel(
    dims,
    partial_ref, tokens_ref, first_gain_ref, gain_ref, routes_ref, group_ref, fine_ref, mix_ref,
    dg_hbm, du_hbm, dd_hbm, eg_hbm, eu_hbm, ed_hbm, key_hbm, value_hbm,
    out_ref, key_out, value_out,
    dg, du, dd, eg, eu, ed, key_w, value_w, aux_w,
    route_buf, tp_buf, resid_buf, rows_buf, pick_buf, mask_buf, chosen_buf,
    gsend, grecv, usend, urecv, esend, erecv, asend, arecv,
    hid_buf, ehid_buf, dense_buf, eout_buf, fin_send, fin_recv,
    load_sem, rt_s, rt_r, tp_s, tp_r, row_s, row_r, pre_s, pre_r, hid_s, hid_r, fin_s, fin_r,
):
    E, T, S, W, U, F, slots, per_group, fine_count = dims
    ET = E // T
    RB, CB = ET * S, ET * slots
    me_e, me_t = lax.axis_index("ep"), lax.axis_index("tp")

    loads = [
        pltpu.make_async_copy(src, dst, load_sem.at[i])
        for i, (src, dst) in enumerate(
            [(dg_hbm, dg), (du_hbm, du), (eg_hbm, eg), (eu_hbm, eu), (dd_hbm, dd), (ed_hbm, ed),
             (key_hbm, key_w), (value_hbm, value_w)]
        )
    ]
    for load in loads:
        load.start()

    feature_rows = pl.ds(pl.multiple_of(me_t * W, LANES), W)
    fine_at = 16
    mix = fine_at + (fine_count + 15) // 16 * 16
    mix_w = mix_ref[:, feature_rows]
    high = mix_w.astype(jnp.bfloat16)
    aux_w[...] = jnp.zeros_like(aux_w)
    aux_w[:GROUPS] = group_ref[:, feature_rows]
    aux_w[fine_at : fine_at + fine_count] = fine_ref[:, feature_rows]
    aux_w[mix : mix + 1] = high
    aux_w[mix + 16 : mix + 17] = (mix_w - high.astype(jnp.float32)).astype(jnp.bfloat16)
    route_buf[0] = jnp.full((8, LANES), -1.0, jnp.float32)
    route_buf[0, :TOP_K, :S] = routes_ref[...].astype(jnp.float32)

    barrier = pltpu.get_barrier_semaphore()

    def greet(d, carry):
        pl.semaphore_signal(
            barrier, inc=1, device_id={"ep": lax.rem(me_e + d, E)}, device_id_type=MESH
        )
        return carry

    lax.fori_loop(1, E, greet, 0)
    for j in range(1, T):
        pl.semaphore_signal(
            barrier, inc=1, device_id={"tp": lax.rem(me_t + j, T)}, device_id_type=MESH
        )
    pl.semaphore_wait(barrier, E - 1 + T - 1)

    def remote(src, dst, send, recv, device):
        return pltpu.make_async_remote_copy(
            src_ref=src, dst_ref=dst, send_sem=send, recv_sem=recv,
            device_id=device, device_id_type=MESH,
        )

    def feature_block(index):
        return pl.ds(pl.multiple_of(index * W, LANES), W)

    tp_copies = []
    for j in range(1, T):
        peer = lax.rem(me_t + j, T)
        tp_copies.append(
            remote(
                partial_ref.at[:, feature_block(peer)], tp_buf.at[j - 1],
                tp_s.at[j - 1], tp_r.at[j - 1], {"tp": peer},
            )
        )
        tp_copies[-1].start()

    def route_copy(d):
        return remote(
            route_buf.at[0], route_buf.at[d], rt_s.at[d], rt_r.at[d], {"ep": lax.rem(me_e + d, E)}
        )

    def row_copy(d):
        return remote(
            rows_buf.at[0], rows_buf.at[d], row_s.at[d], row_r.at[d], {"ep": lax.rem(me_e + d, E)}
        )

    def fin_copy(d):
        return remote(
            fin_send.at[d], fin_recv.at[d], fin_s.at[d], fin_r.at[d],
            {"ep": lax.rem(me_e - d + E, E)},
        )

    def each(first, body):
        def step(d, carry):
            body(d)
            return carry

        lax.fori_loop(first, E, step, 0)

    each(1, lambda d: route_copy(d).start())

    def dot(a, b):
        return jnp.dot(a, b, preferred_element_type=jnp.float32)

    def dot_t(a, b):
        return lax.dot_general(
            a, b, (((1,), (1,)), ((), ())), preferred_element_type=jnp.float32
        )

    for load in loads[6:]:
        load.wait()
    h_first = normed(tokens_ref[...], first_gain_ref[...]).astype(jnp.bfloat16)
    key_out[...] = dot_t(h_first, key_w[...]).astype(jnp.bfloat16)
    value_out[...] = dot_t(h_first, value_w[...]).astype(jnp.bfloat16)

    gain = gain_ref[:, feature_block(me_t)]
    total = tokens_ref[:, feature_block(me_t)].astype(jnp.float32)
    total = total + partial_ref[:, feature_block(me_t)].astype(jnp.float32)
    for j in range(1, T):
        tp_copies[j - 1].wait_recv()
        total = total + tp_buf[j - 1].astype(jnp.float32)
    resid_buf[...] = total
    rows_buf[0] = (total * gain).astype(jnp.bfloat16)

    partner = me_t + 1 - 2 * lax.rem(me_t, 2)
    across = lax.rem(me_t + T // 2, T)
    opposite = lax.rem(partner + T // 2, T)

    def block_of(owner, body):
        def step(i, carry):
            body(owner * ET + i)
            return carry

        lax.fori_loop(0, ET, step, 0)

    def from_others(body):
        def guarded(d):
            @pl.when(d > 0)
            def _():
                body(d)

        return guarded

    for owner in (opposite, across, partner, me_t):
        block_of(owner, from_others(lambda d: row_copy(d).start()))

    each(1, lambda d: route_copy(d).wait_recv())
    own = me_e.astype(jnp.float32)
    before = (
        lax.broadcasted_iota(jnp.int32, (LANES, LANES), 0)
        < lax.broadcasted_iota(jnp.int32, (LANES, LANES), 1)
    ).astype(jnp.float32).astype(jnp.bfloat16)
    slot_iota = lax.broadcasted_iota(jnp.int32, (slots, LANES), 0).astype(jnp.float32)
    lane_iota = lax.broadcasted_iota(jnp.int32, (slots, LANES), 1).astype(jnp.float32)

    def pick(d):
        named = route_buf[d]
        hits = jnp.where(named == own, 1.0, 0.0)
        ranks = jnp.dot(hits.astype(jnp.bfloat16), before, preferred_element_type=jnp.float32)
        rank = jnp.sum(ranks, axis=0, keepdims=True)
        hit = jnp.sum(hits, axis=0, keepdims=True)
        picks = jnp.where(slot_iota == rank, 1.0, 0.0) * hit
        pick_buf[d] = picks
        mask = jnp.zeros((slots, LANES), jnp.float32)
        for i in range(TOP_K):
            chosen = jnp.sum(picks * named[i : i + 1, :], axis=1, keepdims=True)
            mask = jnp.where(lane_iota == chosen + float(fine_at), 1.0, mask)
        mask_buf[d] = mask

    each(0, pick)

    def gather(d):
        chosen_buf[d] = jnp.dot(
            pick_buf[d][:, :S].astype(jnp.bfloat16), rows_buf[d],
            preferred_element_type=jnp.float32,
        )

    def gather_arrived(d):
        @pl.when(d > 0)
        def _():
            row_copy(d).wait_recv()

        gather(d)

    for load in loads[:4]:
        load.wait()

    inverse = 1.0 / gain

    def partials(owner):
        block_of(owner, gather_arrived)
        rows = rows_buf[pl.ds(owner * ET, ET)].astype(jnp.float32).reshape(RB, W)
        picked = chosen_buf[pl.ds(owner * ET, ET)].reshape(CB, W)
        both = jnp.concatenate([rows, picked], axis=0)
        scaled = both * inverse
        squares = jnp.sum(scaled * scaled, axis=1, keepdims=True)
        rows, picked = rows.astype(jnp.bfloat16), picked.astype(jnp.bfloat16)
        lanes = lax.broadcasted_iota(jnp.int32, (RB + CB, LANES), 1)
        aux = dot_t(both.astype(jnp.bfloat16), aux_w[...]) + jnp.where(lanes == LANES - 1, squares, 0.0)
        return rows, picked, aux

    pairs = [(gsend, grecv), (usend, urecv), (esend, erecv), (asend, arecv)]
    pre_copies = {}

    def send(n, k, value, device):
        src, dst = pairs[k]
        src[n] = value.astype(src.dtype)
        pre_copies[n, k] = remote(
            src.at[n], dst.at[n], pre_s.at[n, k], pre_r.at[n, k], {"tp": device}
        )
        pre_copies[n, k].start()

    def products(owner, consume):
        rows, picked, aux = partials(owner)
        consume(0, dot(rows, dg[...]))
        consume(1, dot(rows, du[...]))
        consume(2, jnp.concatenate([dot(picked, eg[...]), dot(picked, eu[...])], axis=1))
        consume(3, aux)

    def arrived(n, k):
        pre_copies[n, k].wait_recv()
        return pairs[k][1][n].astype(jnp.float32)

    products(opposite, lambda k, value: send(0, k, value, partner))
    products(across, lambda k, value: send(1, k, value + arrived(0, k), across))
    products(partner, lambda k, value: send(2, k, value, partner))
    kept = {}

    def keep(k, value):
        kept[k] = value + arrived(2, k)

    products(me_t, keep)
    gate, up, both_e, aux = [kept[k] + arrived(1, k) for k in range(4)]
    egate, eup = both_e[:, :F], both_e[:, F:]
    scale = lax.rsqrt(aux[:, LANES - 1 :] / (T * W) + norm_eps)
    logits = aux * scale
    mix_gate = jax.nn.sigmoid(logits[:RB, mix : mix + 1] + logits[:RB, mix + 16 : mix + 17])
    dense_scale, slot_scale = scale[:RB], scale[RB:]
    gate, up = gate * dense_scale, up * dense_scale
    hid_buf[me_t] = (jax.nn.silu(gate) * up * mix_gate).astype(jnp.bfloat16)

    slot_logits = logits[RB:]
    lanes = lax.broadcasted_iota(jnp.int32, (CB, LANES), 1)

    def at_lane(lane):
        return jnp.sum(jnp.where(lanes == lane, slot_logits, 0.0), axis=1, keepdims=True)

    own_group, own_fine = at_lane(me_e // per_group), at_lane(me_e + fine_at)
    named = mask_buf[pl.ds(me_t * ET, ET)].reshape(CB, LANES)

    def share(inside, own_logit):
        terms = jnp.exp(jnp.where(inside, slot_logits - own_logit, -jnp.inf))
        return 1.0 / jnp.sum(terms, axis=1, keepdims=True)

    shares = share(lanes < GROUPS, own_group) * share(
        (named > 0.0) | (lanes == me_e + fine_at), own_fine
    )
    egate, eup = egate * slot_scale, eup * slot_scale
    ehid_buf[me_t] = (jax.nn.silu(egate) * eup * shares).astype(jnp.bfloat16)

    def hid_copy(n, k, owner, device):
        buf = (hid_buf, ehid_buf)[k]
        return remote(
            buf.at[owner], buf.at[owner], hid_s.at[n, k], hid_r.at[n, k], {"tp": device}
        )

    hid_copies = {}
    for n, (owner, device) in enumerate([(me_t, across), (me_t, partner), (across, partner)]):
        for k in range(2):
            hid_copies[n, k] = hid_copy(n, k, owner, device)
    for n in range(2):
        for k in range(2):
            hid_copies[n, k].start()
    for load in loads[4:6]:
        load.wait()

    def output_of(d):
        back = pick_buf[d].T[:S].astype(jnp.bfloat16)
        return dense_buf[d] + dot(back, eout_buf[d].astype(jnp.bfloat16))

    def finish(d):
        fin_send[d] = output_of(d).astype(jnp.bfloat16)
        fin_copy(d).start()

    def block_out(owner):
        blocks = pl.ds(owner * ET, ET)
        dense_buf[blocks] = dot(hid_buf[owner], dd[...]).reshape(ET, S, W)
        eout_buf[blocks] = dot(ehid_buf[owner], ed[...]).reshape(ET, slots, W)
        block_of(owner, from_others(finish))

    block_out(me_t)
    for k in range(2):
        hid_copies[1, k].wait_recv()
    block_out(partner)
    for k in range(2):
        hid_copies[0, k].wait_recv()
        hid_copies[2, k].start()
    block_out(across)
    for k in range(2):
        hid_copies[2, k].wait_recv()
    block_out(opposite)
    resid_buf[...] += output_of(0)

    def collect(d):
        fin_copy(d).wait_recv()
        resid_buf[...] += fin_recv[d].astype(jnp.float32)

    each(1, collect)
    out_ref[...] = resid_buf[...].astype(jnp.bfloat16)

    for copy in tp_copies + list(pre_copies.values()) + list(hid_copies.values()):
        copy.wait_send()
    each(1, lambda d: route_copy(d).wait_send())
    each(1, lambda d: row_copy(d).wait_send())
    each(1, lambda d: fin_copy(d).wait_send())


def tail(partial, tokens, first_gain, gain, w_key, w_value, routes, w_group, w_fine, w_mix, dg, du, dd, eg, eu, ed):
    E, T = lax.axis_size("ep"), lax.axis_size("tp")
    S, D = tokens.shape
    W, U = dg.shape
    F = eg.shape[1]
    per_group = E // GROUPS
    capacity = max(2, (S + per_group - 1) // per_group)
    slots = (capacity + 7) // 8 * 8
    ET = E // T
    RB, CB = ET * S, ET * slots
    KD = w_key.shape[1]
    bf16, f32 = jnp.bfloat16, jnp.float32
    vmem = pl.BlockSpec(memory_space=pltpu.VMEM)
    anywhere = pl.BlockSpec(memory_space=pltpu.HBM)
    dma = pltpu.SemaphoreType.DMA
    dims = (E, T, S, W, U, F, slots, per_group, w_fine.shape[1])
    return pl.pallas_call(
        functools.partial(tail_kernel, dims),
        out_shape=(
            jax.ShapeDtypeStruct((S, W), bf16),
            jax.ShapeDtypeStruct((S, KD), bf16),
            jax.ShapeDtypeStruct((S, KD), bf16),
        ),
        in_specs=[vmem] * 8 + [anywhere] * 8,
        out_specs=(vmem, vmem, vmem),
        scratch_shapes=[
            pltpu.VMEM((W, U), bf16), pltpu.VMEM((W, U), bf16), pltpu.VMEM((U, W), bf16),
            pltpu.VMEM((W, F), bf16), pltpu.VMEM((W, F), bf16), pltpu.VMEM((F, W), bf16),
            pltpu.VMEM((KD, D), bf16), pltpu.VMEM((KD, D), bf16), pltpu.VMEM((LANES, W), bf16),
            pltpu.VMEM((E, 8, LANES), f32),
            pltpu.VMEM((T - 1, S, W), bf16),
            pltpu.VMEM((S, W), f32),
            pltpu.VMEM((E, S, W), bf16),
            pltpu.VMEM((E, slots, LANES), f32),
            pltpu.VMEM((E, slots, LANES), f32),
            pltpu.VMEM((E, slots, W), f32),
            pltpu.VMEM((3, RB, U), bf16), pltpu.VMEM((3, RB, U), bf16),
            pltpu.VMEM((3, RB, U), bf16), pltpu.VMEM((3, RB, U), bf16),
            pltpu.VMEM((3, CB, 2 * F), bf16), pltpu.VMEM((3, CB, 2 * F), bf16),
            pltpu.VMEM((3, RB + CB, LANES), f32), pltpu.VMEM((3, RB + CB, LANES), f32),
            pltpu.VMEM((T, RB, U), bf16), pltpu.VMEM((T, CB, F), bf16),
            pltpu.VMEM((E, S, W), f32), pltpu.VMEM((E, slots, W), f32),
            pltpu.VMEM((E, S, W), bf16), pltpu.VMEM((E, S, W), bf16),
            dma((8,)), dma((E,)), dma((E,)), dma((T - 1,)), dma((T - 1,)), dma((E,)), dma((E,)),
            dma((3, 4)), dma((3, 4)), dma((3, 2)), dma((3, 2)),
            dma((E,)), dma((E,)),
        ],
        compiler_params=pltpu.CompilerParams(
            collective_id=0, has_side_effects=True, vmem_limit_bytes=48 * 1024 * 1024
        ),
        name="tail",
    )(
        partial, tokens, first_gain[None, :], gain[None, :], routes.T, w_group.T, w_fine.T,
        w_mix[None, :], dg, du, dd, eg, eu, ed, w_key.T, w_value.T,
    )


def shards(
    tokens,
    norm_attn,
    w_query,
    w_key,
    w_value,
    w_out,
    head_bias,
    key_cache,
    value_cache,
    lengths,
    norm_ffn,
    w_group,
    w_fine,
    routes,
    e_gate,
    e_up,
    e_down,
    d_gate,
    d_up,
    d_down,
    w_mix,
):
    seq_count = tokens.shape[0]
    kv_local = key_cache.shape[1]
    head_dim = key_cache.shape[3]
    h_first = normed(tokens, norm_attn).astype(jnp.bfloat16)
    queries = jnp.dot(h_first, w_query, preferred_element_type=jnp.float32).astype(jnp.bfloat16)
    heads_out = stick_read(
        queries.reshape(seq_count, -1, head_dim),
        jnp.swapaxes(key_cache[:, 0], 1, 2), jnp.swapaxes(value_cache[:, 0], 1, 2),
        lengths, head_bias,
    )
    partial_value = jnp.dot(heads_out, w_out, preferred_element_type=jnp.float32).astype(
        jnp.bfloat16
    )
    mixed, new_keys, new_values = tail(
        partial_value, tokens, norm_attn, norm_ffn, w_key, w_value, routes, w_group, w_fine, w_mix,
        d_gate, d_up, d_down, e_gate[0], e_up[0], e_down[0],
    )
    return (
        mixed,
        new_keys.reshape(seq_count, kv_local, head_dim),
        new_values.reshape(seq_count, kv_local, head_dim),
    )


def solution(mesh):
    placed = (
        P("ep", None),
        P(),
        P(None, "tp"),
        P(None, "tp"),
        P(None, "tp"),
        P("tp", None),
        P("tp"),
        P("ep", "tp", None, None),
        P("ep", "tp", None, None),
        P("ep"),
        P(),
        P(),
        P(),
        P("ep", None),
        P("ep", "tp", None),
        P("ep", "tp", None),
        P("ep", None, "tp"),
        P("tp", "ep"),
        P("tp", "ep"),
        P("ep", "tp"),
        P(),
    )
    return jax.shard_map(
        shards,
        mesh=mesh,
        in_specs=placed,
        out_specs=(P("ep", "tp"), P("ep", "tp", None), P("ep", "tp", None)),
        check_vma=False,
    )
```

time: 74.5 us -> 59.5 us (0.80)
  matrix products: 13 us -> 3.31 us
  local copies, waits for them, and re-layouts: 13.1 us -> 9.47 us
  other arithmetic: 2.76 us -> 1.18 us
    dot_general x6 -> x0, matrix products: 8.97 us -> none  [the longest x1 3.32 us: stick_read(): jnp.einsum('bkgs,bksd->bkgd', weights.astype(jnp.bfloat16), values, prefe...]
    unnamed x38 -> x35, local copies, waits for them, and re-layouts: 9.31 us -> 7.15 us
    reduce_sum x1 -> x0, other arithmetic: 1.43 us -> none  [suffix_sums(): jnp.sum(shaped, axis=-1)]
    pad x2 -> x0, local copies, waits for them, and re-layouts: 1.21 us -> none  [the longest x1 1.2 us: tail(): jnp.pad(aux_w, ((0, 0), (0, LANES - aux_w.shape[1]))).reshape(T, W, LANES)]
    dot_general x1, matrix products: 1.98 us -> 1.21 us  [shards(): jnp.dot(heads_out, w_out, preferred_element_type=jnp.float32)]
    pallas_call x1 -> x2, Pallas kernels: 44.3 us -> 44.2 us  [the longest x1 36.9 us: tail(): pl.pallas_call(functools.partial(tail_kernel, dims), out_shape=(jax.Shape...]
where the time goes in v2:
time: 59.5 us; the launch traced here: 59 us
  Pallas kernels  44.2 us (74%)
  local copies, waits for them, and re-layouts  9.47 us (16%)
  matrix products  3.31 us (6%)
  other arithmetic  1.18 us (2%)
  between operations  0.78 us (1%)
    pallas_call x1, Pallas kernels, tail(): pl.pallas_call(functools.partial(tail_kernel, dims), out_shape=(jax.Shape...  36.9 us
    pallas_call x1, Pallas kernels, stick_read(): pl.pallas_call(functools.partial(stick_kernel, batch, heads), grid=(count...  7.38 us
    unnamed x35, local copies, waits for them, and re-layouts  7.15 us
    dot_general x1, matrix products, shards(): jnp.dot(h_first, w_query, preferred_element_type=jnp.float32)  2.1 us
    reshape x1, local copies, waits for them, and re-layouts, stick_read(): return pl.pallas_call(functools.partial(stick_kernel, batch, heads), grid...  1.6 us
    dot_general x1, matrix products, shards(): jnp.dot(heads_out, w_out, preferred_element_type=jnp.float32)  1.21 us

profile of v2, /device:TPU:0, one launch (start us, length us, event | category | flops | bytes accessed | tf_op | source)
XLA Modules:
  0.0 59.0 jit_solution(12522684846241557829)
XLA Ops:
  0.6 0.0 copy-start
  0.6 1.2 %fusion = f32[24]{0:T(128)S(1)} fusion(bf16[24,2048]{1,0:T(8,128)(2,1)} %tokens_ref.1), kind=kLoop, calls=%fused_computation.4 | loop fusion | flops 147432 | bytes 98400 | tf_op jit(solution)/shard_map/reduce_sum | solution.py:18
  1.8 2.1 %convolution_convert_fusion.1 = bf16[24,512]{1,0:T(8,128)(2,1)S(1)} fusion(bf16[2048,512]{1,0:T(8,128)(2,1)} %param.23, bf16[24,2048]{1,0:T(8,128)(2,1)} %tokens_ref.1, f32[2048]{0:T(1024)} %param.22, f32[24]{0:T(128)S(1)} %add_rsqrt_fusion), kind=kOutput, calls=%fused_computation.1 | convolution fusion | flops 50540544 | bytes 2228320 | tf_op jit(solution)/shard_map/dot_general | solution.py:491
  3.9 0.7 %reshape.27.q_ref = bf16[24,8,64]{2,1,0:T(8,128)(2,1)} reshape(bf16[24,512]{1,0:T(8,128)(2,1)S(1)} %convolution_convert_fusion.1) | data formatting | bytes 49152 | tf_op jit(solution)/shard_map/reshape | solution.py:493
  4.6 0.0 copy-start.8
  4.7 7.4 %stick.1 = bf16[24,8,64]{2,1,0:T(8,128)(2,1)} custom-call(s32[24]{0:T(128)} %lengths_ref.1, f32[8]{0:T(128)} %bias_ref.1, bf16[24,8,64]{2,1,0:T(8,128)(2,1)} %reshape.27.q_ref, bf16[24,64,1024]{2,1,0:T(8,128)(2,1)} %bitcast.35, bf16[24,64,1024]{2,1,0:T(8,128)(2,1)} %bitcast.36), custom_call_target="tpu_custom_call" | custom-call | flops 50331648 | bytes 6291456 | tf_op jit(solution)/shard_map/stick/pallas_call | solution.py:73
  12.0 0.0 copy-start.1
  12.0 0.0 copy-start.4
  12.0 0.0 copy-start.10
  12.0 0.0 copy-start.11
  12.1 0.0 copy-start.13
  12.1 1.6 %reshape.28 = bf16[24,512]{1,0:T(8,128)(2,1)} reshape(bf16[24,8,64]{2,1,0:T(8,128)(2,1)} %stick.1) | data formatting | bytes 49152 | tf_op jit(solution)/shard_map/reshape | solution.py:85
  13.7 0.0 copy-done
  13.7 0.0 copy-start.2
  13.7 0.0 copy-start.12
  13.7 0.0 copy-start.14
  13.7 0.0 copy-start.15
  13.7 1.2 %convolution_convert_fusion.partial_ref = bf16[24,2048]{1,0:T(8,128)(2,1)S(1)} fusion(bf16[24,512]{1,0:T(8,128)(2,1)} %reshape.28, bf16[512,2048]{1,0:T(8,128)(2,1)S(1)} %copy-done), kind=kOutput, calls=%fused_computation | convolution fusion | flops 50380800 | bytes 2220032 | tf_op jit(solution)/shard_map/dot_general | solution.py:497
  14.9 0.0 copy-done.8
  14.9 0.0 copy-done.1
  14.9 0.0 copy-done.4
  14.9 0.0 copy-done.10
  15.0 0.0 copy-done.11
  15.0 0.0 copy-done.13
  15.0 0.0 copy-done.2
  15.0 0.0 copy-done.12
  15.0 0.0 copy-done.14
  15.0 0.0 copy-done.15
  15.0 0.0 copy-start.3
  15.0 1.2 %copy-done.3 = bf16[1024,512]{1,0:T(8,128)(2,1)S(1)} copy-done((bf16[1024,512]{1,0:T(8,128)(2,1)S(1)}, bf16[1024,512]{1,0:T(8,128)(2,1)}, u32[]{:S(2)}) %copy-start.3) | copy-done | bytes 1048600
  16.2 0.0 copy-start.5
  16.2 1.0 %copy-done.5 = bf16[1,512,512]{2,1,0:T(8,128)(2,1)S(1)} copy-done((bf16[1,512,512]{2,1,0:T(8,128)(2,1)S(1)}, bf16[1,512,512]{2,1,0:T(8,128)(2,1)}, u32[]{:S(2)}) %copy-start.5) | copy-done | bytes 524312
  17.3 0.0 copy-start.6
  17.3 1.0 %copy-done.6 = bf16[1,512,512]{2,1,0:T(8,128)(2,1)S(1)} copy-done((bf16[1,512,512]{2,1,0:T(8,128)(2,1)S(1)}, bf16[1,512,512]{2,1,0:T(8,128)(2,1)}, u32[]{:S(2)}) %copy-start.6) | copy-done | bytes 524312
  18.3 0.0 copy-start.7
  18.3 1.0 %copy-done.7 = bf16[1,512,512]{2,1,0:T(8,128)(2,1)S(1)} copy-done((bf16[1,512,512]{2,1,0:T(8,128)(2,1)S(1)}, bf16[1,512,512]{2,1,0:T(8,128)(2,1)}, u32[]{:S(2)}) %copy-start.7) | copy-done | bytes 524312
  19.4 0.0 copy-start.9
  19.4 0.9 %copy-done.9 = bf16[2048,64]{0,1:T(8,128)(2,1)S(1)} copy-done((bf16[2048,64]{0,1:T(8,128)(2,1)S(1)}, bf16[2048,64]{0,1:T(8,128)(2,1)}, u32[]{:S(2)}) %copy-start.9) | copy-done | bytes 262168
  20.3 36.9 %tail.1 = (bf16[24,512]{1,0:T(8,128)(2,1)S(1)}, bf16[24,64]{1,0:T(8,128)(2,1)S(1)}, bf16[24,64]{1,0:T(8,128)(2,1)S(1)}) custom-call(bf16[24,2048]{1,0:T(8,128)(2,1)S(1)} %convolution_convert_fusion.partial_ref, bf16[24,2048]{1,0:T(8,128)(2,1)S(1)} %copy-done.4, f32[1,2048]{1,0:T(1,128)S(1)} %bitcast.28, f32[1,2048]{1,0:T(1,128)S(1)} %bitcast.30, ...), custom_call_target="tpu_custom_call" | custom-call | tf_op jit(solution)/shard_map/tail/pallas_call | solution.py:423
  57.2 0.6 %copy.27 = bf16[24,512]{1,0:T(8,128)(2,1)} copy(bf16[24,512]{1,0:T(8,128)(2,1)S(1)} %get-tuple-element.12) | data formatting | bytes 49152
  57.8 0.6 %copy.28 = bf16[24,1,64]{2,0,1:T(8,128)(2,1)} copy(bf16[24,1,64]{2,0,1:T(8,128)(2,1)S(1)} %bitcast.33) | data formatting | bytes 6144
  58.4 0.6 %copy.29 = bf16[24,1,64]{2,0,1:T(8,128)(2,1)} copy(bf16[24,1,64]{2,0,1:T(8,128)(2,1)S(1)} %bitcast.32) | data formatting | bytes 6144
  (1 shorter events, 0.0 us)
Async XLA Ops:
  0.6 13.0 %copy-start = (bf16[512,2048]{1,0:T(8,128)(2,1)S(1)}, bf16[512,2048]{1,0:T(8,128)(2,1)}, u32[]{:S(2)}) copy-start(bf16[512,2048]{1,0:T(8,128)(2,1)} %param.26) | copy-start | bytes 6291460
  4.6 10.3 %copy-start.8 = (bf16[2048,64]{0,1:T(8,128)(2,1)S(1)}, bf16[2048,64]{0,1:T(8,128)(2,1)}, u32[]{:S(2)}) copy-start(bf16[2048,64]{0,1:T(8,128)(2,1)} %param.24) | copy-start | bytes 786436
  12.0 2.9 %copy-start.1 = (bf16[512,1024]{1,0:T(8,128)(2,1)S(1)}, bf16[512,1024]{1,0:T(8,128)(2,1)}, u32[]{:S(2)}) copy-start(bf16[512,1024]{1,0:T(8,128)(2,1)} %dg_hbm.1) | copy-start | bytes 3145732
  12.0 2.9 %copy-start.4 = (bf16[24,2048]{1,0:T(8,128)(2,1)S(1)}, bf16[24,2048]{1,0:T(8,128)(2,1)}, u32[]{:S(2)}) copy-start(bf16[24,2048]{1,0:T(8,128)(2,1)} %tokens_ref.1) | copy-start | bytes 294916
  12.0 2.9 %copy-start.10 = (bf16[2048,8]{0,1:T(8,128)(2,1)S(1)}, bf16[2048,8]{0,1:T(8,128)(2,1)}, u32[]{:S(2)}) copy-start(bf16[2048,8]{0,1:T(8,128)(2,1)} %param.33) | copy-start | bytes 98308
  12.0 2.9 %copy-start.11 = (f32[2048]{0:T(1024)S(1)}, f32[2048]{0:T(1024)}, u32[]{:S(2)}) copy-start(f32[2048]{0:T(1024)} %param.22) | copy-start | bytes 24580
  12.1 2.9 %copy-start.13 = (f32[2048]{0:T(1024)S(1)}, f32[2048]{0:T(1024)}, u32[]{:S(2)}) copy-start(f32[2048]{0:T(1024)} %param.31) | copy-start | bytes 24580
  13.7 1.3 %copy-start.2 = (bf16[512,1024]{1,0:T(8,128)(2,1)S(1)}, bf16[512,1024]{1,0:T(8,128)(2,1)}, u32[]{:S(2)}) copy-start(bf16[512,1024]{1,0:T(8,128)(2,1)} %du_hbm.1) | copy-start | bytes 3145732
  13.7 1.3 %copy-start.12 = (bf16[2048,4]{0,1:T(4,128)(2,1)S(1)}, bf16[2048,4]{0,1:T(4,128)(2,1)}, u32[]{:S(2)}) copy-start(bf16[2048,4]{0,1:T(4,128)(2,1)} %param.32) | copy-start | bytes 49156
  13.7 1.3 %copy-start.14 = (f32[2048]{0:T(1024)S(1)}, f32[2048]{0:T(1024)}, u32[]{:S(2)}) copy-start(f32[2048]{0:T(1024)} %param.41) | copy-start | bytes 24580
  13.7 1.3 %copy-start.15 = (s32[24,2]{0,1:T(2,128)S(1)}, s32[24,2]{0,1:T(2,128)}, u32[]{:S(2)}) copy-start(s32[24,2]{0,1:T(2,128)} %param.34) | copy-start | bytes 580
  15.0 1.2 %copy-start.3 = (bf16[1024,512]{1,0:T(8,128)(2,1)S(1)}, bf16[1024,512]{1,0:T(8,128)(2,1)}, u32[]{:S(2)}) copy-start(bf16[1024,512]{1,0:T(8,128)(2,1)} %dd_hbm.1) | copy-start | bytes 3145732
  16.2 1.0 %copy-start.5 = (bf16[1,512,512]{2,1,0:T(8,128)(2,1)S(1)}, bf16[1,512,512]{2,1,0:T(8,128)(2,1)}, u32[]{:S(2)}) copy-start(bf16[1,512,512]{2,1,0:T(8,128)(2,1)} %param.35) | copy-start | bytes 1572868
  17.3 1.0 %copy-start.6 = (bf16[1,512,512]{2,1,0:T(8,128)(2,1)S(1)}, bf16[1,512,512]{2,1,0:T(8,128)(2,1)}, u32[]{:S(2)}) copy-start(bf16[1,512,512]{2,1,0:T(8,128)(2,1)} %param.36) | copy-start | bytes 1572868
  18.3 1.0 %copy-start.7 = (bf16[1,512,512]{2,1,0:T(8,128)(2,1)S(1)}, bf16[1,512,512]{2,1,0:T(8,128)(2,1)}, u32[]{:S(2)}) copy-start(bf16[1,512,512]{2,1,0:T(8,128)(2,1)} %param.37) | copy-start | bytes 1572868
  19.4 0.9 %copy-start.9 = (bf16[2048,64]{0,1:T(8,128)(2,1)S(1)}, bf16[2048,64]{0,1:T(8,128)(2,1)}, u32[]{:S(2)}) copy-start(bf16[2048,64]{0,1:T(8,128)(2,1)} %param.25) | copy-start | bytes 786436

commit v3 on v2

--- a/solution.py
+++ b/solution.py
@@ -86,6 +86,7 @@
 
 
 LANES = 128
+VMEM_BYTES = 67043328
 MESH = pl.DeviceIdType.MESH
 
 
@@ -112,9 +113,22 @@
              (key_hbm, key_w), (value_hbm, value_w)]
         )
     ]
-    for load in loads:
+    for load in loads[6:] + loads[:6]:
         load.start()
 
+    barrier = pltpu.get_barrier_semaphore()
+
+    def greet(d, carry):
+        pl.semaphore_signal(
+            barrier, inc=1, device_id={"ep": lax.rem(me_e + d, E)}, device_id_type=MESH
+        )
+        return carry
+
+    lax.fori_loop(1, E, greet, 0)
+    for j in range(1, T):
+        pl.semaphore_signal(
+            barrier, inc=1, device_id={"tp": lax.rem(me_t + j, T)}, device_id_type=MESH
+        )
     feature_rows = pl.ds(pl.multiple_of(me_t * W, LANES), W)
     fine_at = 16
     mix = fine_at + (fine_count + 15) // 16 * 16
@@ -127,20 +141,6 @@
     aux_w[mix + 16 : mix + 17] = (mix_w - high.astype(jnp.float32)).astype(jnp.bfloat16)
     route_buf[0] = jnp.full((8, LANES), -1.0, jnp.float32)
     route_buf[0, :TOP_K, :S] = routes_ref[...].astype(jnp.float32)
-
-    barrier = pltpu.get_barrier_semaphore()
-
-    def greet(d, carry):
-        pl.semaphore_signal(
-            barrier, inc=1, device_id={"ep": lax.rem(me_e + d, E)}, device_id_type=MESH
-        )
-        return carry
-
-    lax.fori_loop(1, E, greet, 0)
-    for j in range(1, T):
-        pl.semaphore_signal(
-            barrier, inc=1, device_id={"tp": lax.rem(me_t + j, T)}, device_id_type=MESH
-        )
     pl.semaphore_wait(barrier, E - 1 + T - 1)
 
     def remote(src, dst, send, recv, device):
@@ -452,7 +452,7 @@
             dma((E,)), dma((E,)),
         ],
         compiler_params=pltpu.CompilerParams(
-            collective_id=0, has_side_effects=True, vmem_limit_bytes=48 * 1024 * 1024
+            collective_id=0, has_side_effects=True, vmem_limit_bytes=VMEM_BYTES
         ),
         name="tail",
     )(

time: 59.5 us -> 56.5 us (0.950)
  local copies, waits for them, and re-layouts: 9.47 us -> 5.55 us
  Pallas kernels: 44.2 us -> 45.6 us
    unnamed x35 -> x5, local copies, waits for them, and re-layouts: 7.15 us -> 3.92 us
    pallas_call x1, Pallas kernels: 36.9 us -> 38.1 us  [tail(): pl.pallas_call(functools.partial(tail_kernel, dims), out_shape=(jax.Shape...]
    reshape x1, local copies, waits for them, and re-layouts: 1.6 us -> 0.9 us  [stick_read(): return pl.pallas_call(functools.partial(stick_kernel, batch, heads), grid...]
where the time goes in v3:
time: 56.5 us; the launch traced here: 56 us
  Pallas kernels  45.6 us (81%)
  local copies, waits for them, and re-layouts  5.55 us (10%)
  matrix products  3.12 us (6%)
  other arithmetic  1.03 us (2%)
  between operations  0.65 us (1%)
    pallas_call x1, Pallas kernels, tail(): pl.pallas_call(functools.partial(tail_kernel, dims), out_shape=(jax.Shape...  38.1 us
    pallas_call x1, Pallas kernels, stick_read(): pl.pallas_call(functools.partial(stick_kernel, batch, heads), grid=(count...  7.48 us
    unnamed x5, local copies, waits for them, and re-layouts  3.92 us
    dot_general x1, matrix products, shards(): jnp.dot(h_first, w_query, preferred_element_type=jnp.float32)  2.1 us

profile of v3, /device:TPU:0, one launch (start us, length us, event | category | flops | bytes accessed | tf_op | source)
XLA Modules:
  0.0 56.0 jit_solution(1412730055937338171)
XLA Ops:
  0.6 1.0 %fusion = f32[24]{0:T(128)S(1)} fusion(bf16[24,2048]{1,0:T(8,128)(2,1)} %tokens_ref.1), kind=kLoop, calls=%fused_computation.4 | loop fusion | flops 147432 | bytes 98400 | tf_op jit(solution)/shard_map/reduce_sum | solution.py:18
  1.7 2.1 %convolution_convert_fusion.1 = bf16[24,512]{1,0:T(8,128)(2,1)S(1)} fusion(bf16[2048,512]{1,0:T(8,128)(2,1)} %param.23, bf16[24,2048]{1,0:T(8,128)(2,1)} %tokens_ref.1, f32[2048]{0:T(1024)} %param.22, f32[24]{0:T(128)S(1)} %add_rsqrt_fusion), kind=kOutput, calls=%fused_computation.1 | convolution fusion | flops 50540544 | bytes 2228320 | tf_op jit(solution)/shard_map/dot_general | solution.py:491
  3.8 0.7 %reshape.27.q_ref = bf16[24,8,64]{2,1,0:T(8,128)(2,1)} reshape(bf16[24,512]{1,0:T(8,128)(2,1)S(1)} %convolution_convert_fusion.1) | data formatting | bytes 49152 | tf_op jit(solution)/shard_map/reshape | solution.py:493
  4.5 0.0 copy-start
  4.5 7.5 %stick.1 = bf16[24,8,64]{2,1,0:T(8,128)(2,1)} custom-call(s32[24]{0:T(128)} %lengths_ref.1, f32[8]{0:T(128)} %bias_ref.1, bf16[24,8,64]{2,1,0:T(8,128)(2,1)} %reshape.27.q_ref, bf16[24,64,1024]{2,1,0:T(8,128)(2,1)} %bitcast.22, bf16[24,64,1024]{2,1,0:T(8,128)(2,1)} %bitcast.23), custom_call_target="tpu_custom_call" | custom-call | flops 50331648 | bytes 6291456 | tf_op jit(solution)/shard_map/stick/pallas_call | solution.py:73
  12.0 0.9 %reshape.28 = bf16[24,512]{1,0:T(8,128)(2,1)S(1)} reshape(bf16[24,8,64]{2,1,0:T(8,128)(2,1)} %stick.1) | data formatting | bytes 49152 | tf_op jit(solution)/shard_map/reshape | solution.py:85
  12.9 0.0 copy-done
  12.9 1.0 %convolution_convert_fusion.partial_ref = bf16[24,2048]{1,0:T(8,128)(2,1)} fusion(bf16[24,512]{1,0:T(8,128)(2,1)S(1)} %reshape.28, bf16[512,2048]{1,0:T(8,128)(2,1)S(1)} %copy-done), kind=kOutput, calls=%fused_computation | convolution fusion | flops 50380800 | bytes 2220032 | tf_op jit(solution)/shard_map/dot_general | solution.py:497
  13.9 38.1 %tail.1 = (bf16[24,512]{1,0:T(8,128)(2,1)}, bf16[24,64]{1,0:T(8,128)(2,1)}, bf16[24,64]{1,0:T(8,128)(2,1)}) custom-call(bf16[24,2048]{1,0:T(8,128)(2,1)} %convolution_convert_fusion.partial_ref, bf16[24,2048]{1,0:T(8,128)(2,1)} %tokens_ref.1, f32[1,2048]{1,0:T(1,128)} %bitcast.30, f32[1,2048]{1,0:T(1,128)} %bitcast.32, s32[2,24]{1,0:T(2,128)} %bitcast.36, ...), custom_call_target="tpu_custom_call" | custom-call | tf_op jit(solution)/shard_map/tail/pallas_call | solution.py:423
  52.0 1.3 %copy.27 = bf16[24,512]{1,0:T(8,128)(2,1)} copy(bf16[24,512]{1,0:T(8,128)(2,1)} %get-tuple-element.12) | data formatting | bytes 49152
  53.4 1.3 %copy.28 = bf16[24,1,64]{2,0,1:T(8,128)(2,1)} copy(bf16[24,1,64]{2,0,1:T(8,128)(2,1)} %bitcast.35) | data formatting | bytes 6144
  54.7 1.3 %copy.29 = bf16[24,1,64]{2,0,1:T(8,128)(2,1)} copy(bf16[24,1,64]{2,0,1:T(8,128)(2,1)} %bitcast.34) | data formatting | bytes 6144
  (1 shorter events, 0.0 us)
Async XLA Ops:
  4.5 8.4 %copy-start = (bf16[512,2048]{1,0:T(8,128)(2,1)S(1)}, bf16[512,2048]{1,0:T(8,128)(2,1)}, u32[]{:S(2)}) copy-start(bf16[512,2048]{1,0:T(8,128)(2,1)} %param.26) | copy-start | bytes 6291460
